TPU v7x, 32 devices: a whole 2x2x4 slice. The times are simulated.
32 devices in a mesh: sp: 8 (over z, x), tp: 4 (over y, core).
Axes of the slice: x: 2, y: 2, z: 4, core: 2. Of those that a mesh axis runs over, the one named last changes fastest.
Arguments:
- layer_source_vector: bfloat16 [2560, 2048], P('sp', 'tp'), may hold values from -40 to 40
- attention_lane_source: bfloat16 [2560, 1024], P('sp', 'tp'), may hold values from -6 to 6
- result_valve_logits: bfloat16 [2560, 1024], P('sp', 'tp'), may hold values from -6 to 6
- memory_write_matrix: bfloat16 [2560, 512], P('sp'), may hold values from -6 to 6
- memory_query_matrix: bfloat16 [2560, 512], P('sp'), may hold values from -6 to 6
- increment_logits: bfloat16 [2, 2560, 16], P(None, 'sp', 'tp'), may hold values from -3 to 3
- increment_offset: float32 [2, 16], P(None, 'tp'), may hold values from -16 to -3
- log_fade_speed: float32 [2, 16], P(None, 'tp'), may hold values from 0 to 1.4
- extra_log_fade: float32 [2, 2560, 16], P(None, 'sp', 'tp'), may hold values from -3 to 0
- attention_bypass_factor: float32 [16], P('tp'), may hold values from 0.1 to 1.9
- attention_lane_kernel: bfloat16 [5, 1024], P(None, 'tp'), may hold values from -2.5 to 2.5
- memory_write_kernel: bfloat16 [5, 512], replicated, may hold values from -2.5 to 2.5
- memory_query_kernel: bfloat16 [5, 512], replicated, may hold values from -2.5 to 2.5
- cluster_rescale_factor: float32 [1024], P('tp'), may hold values from 0.1 to 1.9
- blender_result_matrix: bfloat16 [1024, 2048], P(None, 'tp'), may hold values from -0.1875 to 0.1875
- specialist_rescale_factor: float32 [2048], P('tp'), may hold values from 0.1 to 1.9
- chosen_specialists: int32 [2560, 2], P('sp'), may hold values from 0 to 7, all different within a row; in each aligned block of 320 rows (0 to 319, 320 to 639, ...) at most 120 rows name the same one
- specialist_shares: float32 [2560, 2], P('sp'), may hold values from 0.25 to 1.25
- specialist_valve_matrix: bfloat16 [8, 2048, 2048], P('sp', None, 'tp'), may hold values from -0.125 to 0.125
- specialist_raising_matrix: bfloat16 [8, 2048, 2048], P('sp', None, 'tp'), may hold values from -0.125 to 0.125
- specialist_lowering_matrix: bfloat16 [8, 2048, 2048], P('sp', None, 'tp'), may hold values from -0.125 to 0.125
- common_valve_matrix: bfloat16 [2048, 2048], P(None, 'tp'), may hold values from -0.125 to 0.125
- common_raising_matrix: bfloat16 [2048, 2048], P(None, 'tp'), may hold values from -0.125 to 0.125
- common_lowering_matrix: bfloat16 [2048, 2048], P(None, 'tp'), may hold values from -0.125 to 0.125
Outputs:
- result: bfloat16 [2560, 2048], P('sp', 'tp')
Inputs may be any that keep to these rules, and one draw needn't show every extreme that they name: `chosen_specialists`: each row names 2 different experts; among the rows of one index of sp no expert is named more than 120 times, a bound that some block reaches there.
All inputs are finite; a program needn't handle non-finite values.
Results may differ from a plain program's by a relative error of at most 0.013.
Values may be sent and summed in bfloat16 or wider, within the bound.
A program may use at most 64 MiB of HBM per device.

v0:
```python
import jax
import jax.numpy as jnp
from jax import lax
from jax.sharding import PartitionSpec as P

D = 2048
HEADS = 16
HEAD_DIM = 64
GROUPS = 4
STATE = 128
CONV = 5


def extended(cells, sides, width):
    for axis, dim in sides:
        count = lax.axis_size(axis)
        ends = count - 1
        head = lax.slice_in_dim(cells, 0, width, axis=dim)
        tail = lax.slice_in_dim(cells, cells.shape[dim] - width, cells.shape[dim], axis=dim)
        cells = jnp.concatenate(
            [
                lax.ppermute(tail, axis, [(i, (i + 1) % count) for i in range(ends)]),
                cells,
                lax.ppermute(head, axis, [((i + 1) % count, i) for i in range(ends)]),
            ],
            axis=dim,
        )
    return cells


def shards(
    layer_source_vector,
    attention_lane_source,
    result_valve_logits,
    memory_write_matrix,
    memory_query_matrix,
    increment_logits,
    increment_offset,
    log_fade_speed,
    extra_log_fade,
    attention_bypass_factor,
    attention_lane_kernel,
    memory_write_kernel,
    memory_query_kernel,
    cluster_rescale_factor,
    blender_result_matrix,
    specialist_rescale_factor,
    chosen_specialists,
    specialist_shares,
    specialist_valve_matrix,
    specialist_raising_matrix,
    specialist_lowering_matrix,
    common_valve_matrix,
    common_raising_matrix,
    common_lowering_matrix,
):
    length = attention_lane_source.shape[0]
    heads_here = increment_offset.shape[1]
    channels = attention_lane_source.shape[1]
    head_size = channels // heads_here
    spread = HEADS // GROUPS
    group = lax.axis_index("tp") * heads_here // spread
    b_own = lax.dynamic_slice_in_dim(memory_write_matrix, group * STATE, STATE, 1)
    c_own = lax.dynamic_slice_in_dim(memory_query_matrix, group * STATE, STATE, 1)
    joined = jnp.concatenate([attention_lane_source, b_own, c_own], axis=1)
    taps = jnp.concatenate(
        [
            attention_lane_kernel,
            lax.dynamic_slice_in_dim(memory_write_kernel, group * STATE, STATE, 1),
            lax.dynamic_slice_in_dim(memory_query_kernel, group * STATE, STATE, 1),
        ],
        axis=1,
    )
    padded = extended(joined, (("sp", 0),), CONV // 2)
    total = jnp.zeros(joined.shape, jnp.float32)
    for offset in range(CONV):
        total = total + padded[offset : offset + length].astype(jnp.float32) * taps[offset].astype(
            jnp.float32
        )
    convolved = jax.nn.silu(total).astype(jnp.bfloat16)
    x_conv = convolved[:, :channels].reshape(length, heads_here, head_size)
    b_conv = convolved[:, channels : channels + STATE]
    c_conv = convolved[:, channels + STATE :]
    increment_lengths = jax.nn.softplus(
        increment_logits.astype(jnp.float32) + increment_offset[:, None, :]
    )
    log_fade_amount = -jnp.exp(log_fade_speed)[:, None, :] * increment_lengths + extra_log_fade
    forward_cum = jnp.cumsum(log_fade_amount[0], axis=0)
    backward_cum = jnp.cumsum(log_fade_amount[1], axis=0) - log_fade_amount[1]
    forward_total = forward_cum[-1]
    backward_total = backward_cum[-1] + log_fade_amount[1][-1]
    scores = lax.dot_general(
        c_conv, b_conv, (((1,), (1,)), ((), ())), preferred_element_type=jnp.float32
    )
    position = jnp.arange(length)
    lower = position[:, None] >= position[None, :]
    upper = position[:, None] <= position[None, :]
    forward_gap = forward_cum.T[:, :, None] - forward_cum.T[:, None, :]
    backward_gap = backward_cum.T[:, None, :] - backward_cum.T[:, :, None]
    forward_part = (
        jnp.where(lower, jnp.exp(jnp.where(lower, forward_gap, 0.0)), 0.0)
        * increment_lengths[0].T[:, None, :]
    )
    backward_part = (
        jnp.where(upper, jnp.exp(jnp.where(upper, backward_gap, 0.0)), 0.0)
        * increment_lengths[1].T[:, None, :]
    )
    mixing = (scores[None] * (forward_part + backward_part)).astype(jnp.bfloat16)
    inner = jnp.einsum("hts,shp->thp", mixing, x_conv, preferred_element_type=jnp.float32)
    forward_scale = jnp.exp(forward_total[None, :] - forward_cum) * increment_lengths[0]
    backward_scale = jnp.exp(backward_cum) * increment_lengths[1]
    scaled = (
        jnp.stack([forward_scale, backward_scale])[..., None] * x_conv.astype(jnp.float32)[None]
    ).astype(jnp.bfloat16)
    own_states = jnp.einsum("dshp,sn->dhpn", scaled, b_conv, preferred_element_type=jnp.float32)
    own_logs = jnp.stack([forward_total, backward_total])
    logs_all, states_all = (
        lax.all_gather(own_logs[None], "sp", axis=0, tiled=True),
        lax.all_gather(own_states[None], "sp", axis=0, tiled=True),
    )
    own_index = lax.axis_index("sp")
    running = jnp.cumsum(logs_all, axis=0)
    before = running - logs_all
    running_own = lax.dynamic_index_in_dim(running, own_index, 0, keepdims=False)
    before_own = lax.dynamic_index_in_dim(before, own_index, 0, keepdims=False)
    block_index = jnp.arange(logs_all.shape[0])[:, None]
    earlier = block_index < own_index
    later = block_index > own_index
    weight_forward = jnp.where(
        earlier, jnp.exp(jnp.where(earlier, before_own[0][None, :] - running[:, 0], 0.0)), 0.0
    )
    weight_backward = jnp.where(
        later, jnp.exp(jnp.where(later, before[:, 1] - running_own[1][None, :], 0.0)), 0.0
    )
    carried_forward = jnp.einsum(
        "jh,jhpn->hpn", weight_forward, states_all[:, 0], precision=lax.Precision.HIGHEST
    )
    carried_backward = jnp.einsum(
        "jh,jhpn->hpn", weight_backward, states_all[:, 1], precision=lax.Precision.HIGHEST
    )
    carried = jnp.stack([carried_forward, carried_backward]).astype(jnp.bfloat16)
    readout = jnp.einsum("tn,dhpn->dthp", c_conv, carried, preferred_element_type=jnp.float32)
    mixer = (
        inner
        + jnp.exp(forward_cum)[..., None] * readout[0]
        + jnp.exp(backward_total[None, :] - backward_cum)[..., None] * readout[1]
        + attention_bypass_factor[None, :, None] * x_conv.astype(jnp.float32)
    )
    gated = mixer * jax.nn.silu(result_valve_logits.astype(jnp.float32)).reshape(
        length, heads_here, head_size
    )
    squares = jnp.sum(gated * gated, axis=(1, 2))
    group_marks = (jnp.arange(GROUPS) == group).astype(jnp.float32)
    group_sums = lax.psum(squares[:, None] * group_marks[None, :], "tp")
    own_sum = lax.dynamic_index_in_dim(group_sums, group, 1, keepdims=False)
    scale = lax.rsqrt(own_sum / (spread * HEAD_DIM) + 1e-06)
    normed = (
        gated.reshape(length, channels) * scale[:, None] * cluster_rescale_factor[None, :]
    ).astype(jnp.bfloat16)
    projected = jnp.dot(
        lax.all_gather(normed, "tp", axis=1, tiled=True),
        blender_result_matrix,
        preferred_element_type=jnp.float32,
    )
    after_mixer = (layer_source_vector.astype(jnp.float32) + projected).astype(jnp.bfloat16)
    resid = after_mixer.astype(jnp.float32)
    total_squares = lax.psum(jnp.sum(resid * resid, axis=1), "tp")
    features = (
        resid * lax.rsqrt(total_squares / D + 1e-06)[:, None] * specialist_rescale_factor[None, :]
    ).astype(jnp.bfloat16)
    full_features = lax.all_gather(features, "tp", axis=1, tiled=True)
    shared_hidden = (
        jax.nn.silu(jnp.dot(full_features, common_valve_matrix, preferred_element_type=jnp.float32))
        * jnp.dot(full_features, common_raising_matrix, preferred_element_type=jnp.float32)
    ).astype(jnp.bfloat16)
    top = chosen_specialists.shape[1]
    experts = lax.axis_size("sp")
    capacity = 3 * length * top // (2 * experts)
    flat = chosen_specialists.reshape(-1)
    one_hot = (flat[:, None] == jnp.arange(experts, dtype=jnp.int32)[None, :]).astype(jnp.int32)
    rank = jnp.sum((jnp.cumsum(one_hot, axis=0) - one_hot) * one_hot, axis=1)
    slot = flat * capacity + rank
    token = jnp.arange(length * top, dtype=jnp.int32) // top
    owner = jnp.zeros((experts * capacity,), jnp.int32).at[slot].set(token)
    filled = jnp.zeros((experts * capacity,), jnp.bool_).at[slot].set(True)
    outgoing = jnp.where(
        filled[:, None], jnp.take(full_features, owner, axis=0), jnp.zeros((), jnp.bfloat16)
    ).reshape(experts, capacity, -1)
    arrived = lax.all_to_all(outgoing, "sp", split_axis=0, concat_axis=0, tiled=True)
    arrived = arrived.reshape(-1, arrived.shape[2])
    expert_hidden = (
        jax.nn.silu(
            jnp.dot(arrived, specialist_valve_matrix[0], preferred_element_type=jnp.float32)
        )
        * jnp.dot(arrived, specialist_raising_matrix[0], preferred_element_type=jnp.float32)
    ).astype(jnp.bfloat16)
    expert_all, shared_all = (
        lax.all_gather(expert_hidden, "tp", axis=1, tiled=True),
        lax.all_gather(shared_hidden, "tp", axis=1, tiled=True),
    )
    expert_out = jnp.dot(
        expert_all, specialist_lowering_matrix[0], preferred_element_type=jnp.float32
    ).astype(jnp.bfloat16)
    shared_out = jnp.dot(
        shared_all, common_lowering_matrix, preferred_element_type=jnp.float32
    ).astype(jnp.bfloat16)
    returned = lax.all_to_all(
        expert_out.reshape(experts, capacity, -1), "sp", split_axis=0, concat_axis=0, tiled=True
    )
    picked = jnp.take(returned.reshape(experts * capacity, -1), slot, axis=0).astype(jnp.float32)
    picked = picked.reshape(length, top, -1)
    routed = jnp.sum(picked * specialist_shares[:, :, None], axis=1)
    return (resid + shared_out.astype(jnp.float32) + routed).astype(jnp.bfloat16)


def solution(mesh):
    return jax.shard_map(
        shards,
        mesh=mesh,
        in_specs=(
            P("sp", "tp"),
            P("sp", "tp"),
            P("sp", "tp"),
            P("sp", None),
            P("sp", None),
            P(None, "sp", "tp"),
            P(None, "tp"),
            P(None, "tp"),
            P(None, "sp", "tp"),
            P("tp"),
            P(None, "tp"),
            P(),
            P(),
            P("tp"),
            P(None, "tp"),
            P("tp"),
            P("sp", None),
            P("sp", None),
            P("sp", None, "tp"),
            P("sp", None, "tp"),
            P("sp", None, "tp"),
            P(None, "tp"),
            P(None, "tp"),
            P(None, "tp"),
        ),
        out_specs=P("sp", "tp"),
        check_vma=False,
    )
```

profile of v0, /device:TPU:0, one launch (start us, length us, event | category | flops | bytes accessed | tf_op | source)
XLA Modules:
  0.0 324.7 jit_solution(13852109089649036000)
XLA Ops:
  8.6 4.9 %collective-permute-start = (bf16[2,512]{1,0:T(2,128)(2,1)S(1)}, bf16[2,512]{1,0:T(2,128)(2,1)S(1)}, u32[]{:S(2)}, u32[]{:S(2)}) collective-permute-start(bf16[2,512]{1,0:T(2,128)(2,1)S(1)} %get-tuple-element.13), channel_id=1, source_target_pairs={{0,4},{4,8},{8,12},{12,16},{16,20},{20,24},{24,28},{1,5},{5,9},{9,... | collective-permute-start | bytes 6152 | tf_op jit(solution)/shard_map/ppermute | solution.py:22
  13.5 1.3 collective-permute-start.1
  17.8 1.2 reduce-window.20
  19.6 1.2 reduce-window.24
  24.7 22.0 %all-gather.2 = f32[8,2,4]{2,1,0:T(2,128)S(1)} all-gather(f32[1,2,4]{2,1,0:T(2,128)S(1)} %bitcast.213), channel_id=2, replica_groups=mesh['sp'=8,'tp'=4] {'sp'}, dimensions={0}, use_global_device_ids=true | all-gather | bytes 288 | tf_op jit(solution)/shard_map/all_gather | solution.py:118
  49.2 26.8 %all-gather.14.cloned.1.call-done = f32[16,4,64,128]{3,2,1,0:T(8,128)} async-done(((f32[2,4,64,128]{3,2,1,0:T(8,128)}), f32[16,4,64,128]{3,2,1,0:T(8,128)}) %all-gather.14.cloned.1.call-update) | async-done | bytes 2097168 | tf_op jit(solution)/shard_map/all_gather | solution.py:119
  76.0 1.7 slice_bitcast_fusion.1
  77.7 1.5 fusion.24
  79.2 1.5 fusion.22
  81.1 1.7 multiply_reduce_fusion.2
  82.8 5.7 %psum.14 = f32[320,4]{0,1:T(4,128)S(1)} all-reduce(f32[320,4]{0,1:T(4,128)S(1)} %broadcast_multiply_fusion), channel_id=1, replica_groups=mesh['sp'=8,'tp'=4] {'tp'}, use_global_device_ids=true, to_apply=%region_6.7 | all-reduce | flops 1280 | bytes 10240 | tf_op jit(solution)/shard_map/psum | solution.py:154
  88.7 8.9 %all_gather.20 = bf16[320,1024]{0,1:T(8,128)(2,1)S(1)} all-gather(bf16[320,256]{0,1:T(8,128)(2,1)S(1)} %fusion.39), channel_id=1, replica_groups=mesh['sp'=8,'tp'=4] {'tp'}, dimensions={1}, use_global_device_ids=true | all-gather | bytes 819200 | tf_op jit(solution)/shard_map/all_gather | solution.py:161
  97.6 1.9 multiply_reduce_fusion.1
  99.5 6.4 %psum.15 = f32[320]{0:T(512)S(1)} all-reduce(f32[320]{0:T(512)S(1)} %get-tuple-element.33), channel_id=1, replica_groups=mesh['sp'=8,'tp'=4] {'tp'}, use_global_device_ids=true, to_apply=%region_8.9 | all-reduce | flops 320 | bytes 2560 | tf_op jit(solution)/shard_map/psum | solution.py:167
  107.3 1.4 reduce-window.26
  109.6 4.3 %scatter_custom_fusion.1 = s32[960]{0:T(1024)S(1)} fusion(s32[640]{0:T(1024)S(1)} %fusion.63, s32[640]{0:T(1024)S(1)} %add_select_fusion, s32[]{:T(128)} %constant.100.clone.1), kind=kCustom, calls=%fused_computation.146 | custom fusion | bytes 3844 | tf_op jit(solution)/shard_map/scatter | solution.py:184
  114.0 2.9 scatter_custom_fusion
  117.1 6.4 %all-gather.8.cloned.1.call-done = bf16[320,2048]{1,0:T(8,128)(2,1)} async-done(((bf16[320,512]{1,0:T(8,128)(2,1)}), bf16[320,2048]{1,0:T(8,128)(2,1)}) %all-gather.8.cloned.1.call-update) | async-done | bytes 1310736 | tf_op jit(solution)/shard_map/all_gather | solution.py:171
  123.5 10.2 %gather_fusion = bf16[960,2048]{1,0:T(8,128)(2,1)} fusion(bf16[320,2048]{1,0:T(8,128)(2,1)} %all-gather.8.cloned.1.call-done, s32[1024]{0:T(1024)S(1)} %pad_clamp_fusion.1), kind=kCustom, calls=%fused_computation | custom fusion | bytes 7868160 | tf_op jit(solution)/shard_map/jit(_take)/gather | solution.py:187
  133.7 2.5 select_select_fusion
  136.2 93.2 %all_to_all.10 = bf16[8,120,2048]{2,1,0:T(8,128)(2,1)S(1)} all-to-all(bf16[8,120,2048]{2,1,0:T(8,128)(2,1)S(1)} %select_select_fusion), channel_id=1, replica_groups=mesh['sp'=8,'tp'=4] {'sp'}, dimensions={0} | all-to-all | bytes 7864320 | tf_op jit(solution)/shard_map/all_to_all | solution.py:189
  229.4 2.2 fusion.4
  231.6 3.4 %multiply_convert_fusion = bf16[960,512]{1,0:T(8,128)(2,1)} fusion(f32[960,512]{1,0:T(8,128)S(1)} %fusion.4, bf16[960,2048]{1,0:T(8,128)(2,1)S(1)} %bitcast.190, bf16[1,2048,512]{2,1,0:T(8,128)(2,1)S(1)} %copy-done.12), kind=kOutput, calls=%fused_computation.11 | convolution fusion | flops 2016215040 | bytes 8978432 | tf_op jit(solution)/shard_map/dot_general | solution.py:195
  235.0 3.3 %fusion.83 = f32[320,512]{1,0:T(8,128)} fusion(bf16[320,2048]{1,0:T(8,128)(2,1)S(1)} %copy-done.1, bf16[2048,512]{1,0:T(8,128)(2,1)} %param.45), kind=kOutput, calls=%fused_computation.175 | convolution fusion | flops 671088640 | bytes 4063232 | tf_op jit(solution)/shard_map/dot_general | solution.py:173
  238.3 28.0 %all-gather.12.cloned.1.call-done = bf16[960,2048]{1,0:T(8,128)(2,1)} async-done(((bf16[960,512]{1,0:T(8,128)(2,1)}), bf16[960,2048]{1,0:T(8,128)(2,1)}) %all-gather.12.cloned.1.call-update) | async-done | bytes 3932176 | tf_op jit(solution)/shard_map/all_gather | solution.py:198
  266.3 5.9 %fusion.8 = bf16[960,512]{1,0:T(8,128)(2,1)} fusion(bf16[960,2048]{1,0:T(8,128)(2,1)} %all-gather.12.cloned.1.call-done, bf16[1,2048,512]{2,1,0:T(8,128)(2,1)} %param.44), kind=kOutput, calls=%fused_computation.13 | convolution fusion | flops 2013757440 | bytes 7012352 | tf_op jit(solution)/shard_map/dot_general | solution.py:201
  272.2 5.5 %all-to-all-start.1 = ((bf16[8,120,512]{2,1,0:T(8,128)(2,1)}), bf16[8,120,512]{2,1,0:T(8,128)(2,1)}, u32[]{:S(2)}, u32[]{:S(2)}) async-start(bf16[8,120,512]{2,1,0:T(8,128)(2,1)} %bitcast.192), calls=%async_computation.1 | async-start | bytes 1966080 | tf_op jit(solution)/shard_map/all_to_all | solution.py:207
  278.0 3.3 %fusion.11 = bf16[320,512]{1,0:T(8,128)(2,1)} fusion(bf16[320,2048]{1,0:T(8,128)(2,1)S(1)} %copy-done.1, bf16[2048,512]{1,0:T(8,128)(2,1)} %param.46, f32[320,512]{1,0:T(8,128)} %fusion.83), kind=kOutput, calls=%fused_computation.19 | convolution fusion | flops 672071680 | bytes 4390912 | tf_op jit(solution)/shard_map/dot_general | solution.py:174
  282.6 20.0 %all-to-all-done.1 = bf16[8,120,512]{2,1,0:T(8,128)(2,1)} async-done(((bf16[8,120,512]{2,1,0:T(8,128)(2,1)}), bf16[8,120,512]{2,1,0:T(8,128)(2,1)}, u32[]{:S(2)}, u32[]{:S(2)}) %all-to-all-start.1) | async-done | bytes 983072 | tf_op jit(solution)/shard_map/all_to_all | solution.py:207
  302.6 4.1 %gather_fusion.1 = bf16[640,512]{1,0:T(8,128)(2,1)S(1)} fusion(bf16[960,512]{1,0:T(8,128)(2,1)} %bitcast.60, s32[1024]{0:T(1024)S(1)} %pad_clamp_fusion), kind=kCustom, calls=%fused_computation.1 | custom fusion | bytes 1313280 | tf_op jit(solution)/shard_map/jit(_take)/gather | solution.py:210
  307.0 7.5 %multiply_reduce_fusion = f32[320,512]{1,0:T(8,128)S(1)} fusion(bf16[320,2,512]{2,1,0:T(2,128)(2,1)S(1)} %gather.15, pred[320,2]{1,0:T(8,128)(4,1)S(1)} %copy.101, f32[320,2]{1,0:T(8,128)} %copy.103), kind=kLoop, calls=%fused_computation.14 | loop fusion | flops 1146880 | bytes 1313920 | tf_op jit(solution)/shard_map/reduce_sum | solution.py:212
  314.5 3.7 %fusion.17 = bf16[320,512]{1,0:T(8,128)(2,1)} fusion(f32[320,512]{1,0:T(8,128)S(1)} %multiply_reduce_fusion, f32[320,512]{1,0:T(8,128)} %copy-done.3, bf16[320,2048]{1,0:T(8,128)(2,1)} %all-gather.10.cloned.1.call-done, bf16[2048,512]{1,0:T(8,128)(2,1)} %param.47), kind=kOutput, calls=%fused_computation.26 | convolution fusion | flops 671907840 | bytes 5046272 | tf_op jit(solution)/shard_map/dot_general | solution.py:204
  (127 shorter events, 16.6 us)
Async XLA Ops:
  6.5 222.9 %copy-start = (bf16[1,2048,512]{2,1,0:T(8,128)(2,1)S(1)}, bf16[1,2048,512]{2,1,0:T(8,128)(2,1)}, u32[]{:S(2)}) copy-start(bf16[1,2048,512]{2,1,0:T(8,128)(2,1)} %param.42) | copy-start | bytes 6291460
  6.5 15.9 %copy-start.2 = (bf16[320,256]{1,0:T(8,128)(2,1)S(1)}, bf16[320,256]{1,0:T(8,128)(2,1)}, u32[]{:S(2)}) copy-start(bf16[320,256]{1,0:T(8,128)(2,1)} %param.25) | copy-start | bytes 491524
  6.5 69.5 %all-gather.14.cloned.1.call-start = ((), (), s32[]{:S(2)}) async-start(), calls=%async_computation.5 | async-start | bytes 2359296 | tf_op jit(solution)/shard_map/all_gather | solution.py:119
  8.6 12.7 %collective-permute-start = (bf16[2,512]{1,0:T(2,128)(2,1)S(1)}, bf16[2,512]{1,0:T(2,128)(2,1)S(1)}, u32[]{:S(2)}, u32[]{:S(2)}) collective-permute-start(bf16[2,512]{1,0:T(2,128)(2,1)S(1)} %get-tuple-element.13), channel_id=1, source_target_pairs={{0,4},{4,8},{8,12},{12,16},{16,20},{20,24},{24,28},{1,5},{5,9},{9,... | collective-permute-start | bytes 6152 | tf_op jit(solution)/shard_map/ppermute | solution.py:22
  13.5 7.9 %collective-permute-start.1 = (bf16[2,512]{1,0:T(2,128)(2,1)S(1)}, bf16[2,512]{1,0:T(2,128)(2,1)S(1)}, u32[]{:S(2)}, u32[]{:S(2)}) collective-permute-start(bf16[2,512]{1,0:T(2,128)(2,1)S(1)} %get-tuple-element.14), channel_id=1, source_target_pairs={{4,0},{8,4},{12,8},{16,12},{20,16},{24,20},{28,24},{5,1},{9,5},{13... | collective-permute-start | bytes 6152 | tf_op jit(solution)/shard_map/ppermute | solution.py:24
  22.5 24.4 %copy-start.5 = (bf16[320,256]{1,0:T(8,128)(2,1)S(1)}, bf16[320,256]{1,0:T(8,128)(2,1)}, u32[]{:S(2)}) copy-start(bf16[320,256]{1,0:T(8,128)(2,1)} %param.26) | copy-start | bytes 491524
  24.3 99.2 %all-gather.8.cloned.1.call-start = ((), (), s32[]{:S(2)}) async-start(), calls=%async_computation.2 | async-start | bytes 1638400 | tf_op jit(solution)/shard_map/all_gather | solution.py:171
  77.7 3.3 %copy-start.4 = (f32[320,320]{1,0:T(8,128)S(1)}, f32[320,320]{1,0:T(8,128)}, u32[]{:S(2)}) copy-start(f32[320,320]{1,0:T(8,128)} %fusion.51) | copy-start | bytes 1228804
  77.7 3.3 %copy-start.6 = (pred[320,320]{1,0:T(8,128)(4,1)S(1)}, pred[320,320]{1,0:T(8,128)(4,1)}, u32[]{:S(2)}) copy-start(pred[320,320]{1,0:T(8,128)(4,1)} %get-tuple-element.43) | copy-start | bytes 307204
  77.7 3.3 %copy-start.7 = (pred[320,320]{1,0:T(8,128)(4,1)S(1)}, pred[320,320]{1,0:T(8,128)(4,1)}, u32[]{:S(2)}) copy-start(pred[320,320]{1,0:T(8,128)(4,1)} %get-tuple-element.44) | copy-start | bytes 307204
  77.7 3.3 %copy-start.13 = (f32[4]{0:T(128)S(1)}, f32[4]{0:T(128)}, u32[]{:S(2)}) copy-start(f32[4]{0:T(128)} %param.33) | copy-start | bytes 52
  81.1 7.5 %copy-start.11 = (f32[256]{0:T(256)S(1)}, f32[256]{0:T(256)}, u32[]{:S(2)}) copy-start(f32[256]{0:T(256)} %param.37) | copy-start | bytes 3076
  88.7 17.2 %copy-start.10 = (f32[512]{0:T(512)S(1)}, f32[512]{0:T(512)}, u32[]{:S(2)}) copy-start(f32[512]{0:T(512)} %param.39) | copy-start | bytes 6148
  97.6 9.3 %copy-start.8 = (s32[320,2]{0,1:T(2,128)S(1)}, s32[320,2]{0,1:T(2,128)}, u32[]{:S(2)}) copy-start(s32[320,2]{0,1:T(2,128)} %param.40) | copy-start | bytes 7684
  99.5 7.3 %copy-start.3 = (f32[320,512]{1,0:T(8,128)}, f32[320,512]{1,0:T(8,128)S(1)}, u32[]{:S(2)}) copy-start(f32[320,512]{1,0:T(8,128)S(1)} %get-tuple-element.34) | copy-start | bytes 1966084
  106.8 159.4 %all-gather.12.cloned.1.call-start = ((), (), s32[]{:S(2)}) async-start(), calls=%async_computation.4 | async-start | bytes 4915200 | tf_op jit(solution)/shard_map/all_gather | solution.py:198
  229.4 2.2 copy-start.12
  231.6 3.4 %copy-start.1 = (bf16[320,2048]{1,0:T(8,128)(2,1)S(1)}, bf16[320,2048]{1,0:T(8,128)(2,1)}, u32[]{:S(2)}) copy-start(bf16[320,2048]{1,0:T(8,128)(2,1)} %all-gather.8.cloned.1.call-done) | copy-start | bytes 3932164
  272.2 30.4 %all-to-all-start.1 = ((bf16[8,120,512]{2,1,0:T(8,128)(2,1)}), bf16[8,120,512]{2,1,0:T(8,128)(2,1)}, u32[]{:S(2)}, u32[]{:S(2)}) async-start(bf16[8,120,512]{2,1,0:T(8,128)(2,1)} %bitcast.192), calls=%async_computation.1 | async-start | bytes 1966080 | tf_op jit(solution)/shard_map/all_to_all | solution.py:207
  277.7 4.1 %copy-start.9 = (f32[320,2]{0,1:T(2,128)S(1)}, f32[320,2]{0,1:T(2,128)}, u32[]{:S(2)}) copy-start(f32[320,2]{0,1:T(2,128)} %param.41) | copy-start | bytes 7684
  277.7 36.8 %all-gather.10.cloned.1.call-start = ((), (), s32[]{:S(2)}) async-start(), calls=%async_computation.3 | async-start | bytes 1638400 | tf_op jit(solution)/shard_map/all_gather | solution.py:199
Sparse Core Ops, SparseCore 0:
  24.4 51.5 all-gather.13
  106.9 16.5 all-gather.7
  235.1 31.0 all-gather.11
  281.5 18.3 all-gather.9
where the time goes:
time: 325 us
  blocking collectives  136 us (42%)
  waiting for transfers between devices  81.2 us (25%)
  matrix products  30.6 us (9%)
  local copies, waits for them, and re-layouts  28.9 us (9%)
  other arithmetic  22 us (7%)
  between operations  13.7 us (4%)
  starting transfers between devices  12 us (4%)
    all_to_all x1, blocking collectives, shards(): lax.all_to_all(outgoing, 'sp', split_axis=0, concat_axis=0, tiled=True)  93.2 us
    all_gather x1, waiting for transfers between devices, shards(): lax.all_gather(expert_hidden, 'tp', axis=1, tiled=True)  28 us
    all_gather x1, waiting for transfers between devices, shards(): lax.all_gather(own_states[None], 'sp', axis=0, tiled=True)  26.8 us
    all_gather x1, blocking collectives, shards(): lax.all_gather(own_logs[None], 'sp', axis=0, tiled=True)  22 us
    all_to_all x1, waiting for transfers between devices, shards(): lax.all_to_all(expert_out.reshape(experts, capacity, -1), 'sp', split_axi...  20 us
    gather x1, local copies, waits for them, and re-layouts, shards(): jnp.take(full_features, owner, axis=0)  10.2 us
    all_gather x1, blocking collectives, shards(): lax.all_gather(normed, 'tp', axis=1, tiled=True)  8.87 us
    reduce_sum x1, other arithmetic, shards(): routed = jnp.sum(picked * specialist_shares[:, :, None], axis=1)  7.48 us
  transfers between devices with their start and end apart: 7, of which 4 were waited for; matrix products, arithmetic and copies ran while one was open for 12% of the time, Pallas kernels for 0%

commit v1 on v0

--- a/solution.py
+++ b/solution.py
@@ -1,7 +1,14 @@
+import functools
+
 import jax
 import jax.numpy as jnp
 from jax import lax
+from jax.experimental import pallas as pl
+from jax.experimental.pallas import tpu as pltpu
 from jax.sharding import PartitionSpec as P
+
+MESH = pl.DeviceIdType.MESH
+KERNEL_DEVICES = 32
 
 D = 2048
 HEADS = 16
@@ -26,6 +33,252 @@
             axis=dim,
         )
     return cells
+
+
+def small_mesh():
+    return lax.axis_size("sp") * lax.axis_size("tp") <= KERNEL_DEVICES
+
+
+def greet(axis, peers):
+    barrier = pltpu.get_barrier_semaphore()
+    for a, peer in zip(axis, peers):
+        pl.semaphore_signal(barrier, inc=1, device_id={a: peer}, device_id_type=MESH)
+    pl.semaphore_wait(barrier, len(peers))
+
+
+def remote(src, dst, send, recv, axis, peer):
+    return pltpu.make_async_remote_copy(
+        src_ref=src,
+        dst_ref=dst,
+        send_sem=send,
+        recv_sem=recv,
+        device_id={axis: peer},
+        device_id_type=MESH,
+    )
+
+
+def gather_kernel(n, counts, *refs):
+    m = len(counts)
+    ins, outs = refs[:m], refs[m : 2 * m]
+    send_sem, recv_sem, local_sem = refs[2 * m :]
+    half = n // 2
+    me = lax.axis_index("tp")
+    row, core = me // 2, me % 2
+    sibling = row * 2 + 1 - core
+    onward = [((row + k) % half) * 2 + core for k in range(1, half)]
+    origin = [((row + half - k) % half) * 2 + core for k in range(1, half)]
+    theirs = [((row + half - k) % half) * 2 + 1 - core for k in range(1, half)]
+    greet(["tp"] * half, [sibling] + onward)
+    pieces = []
+    for i, count in enumerate(counts):
+        size = ins[i].shape[0] // count
+        for c in range(count):
+            pieces.append((i, c * size, size))
+
+    def spot(i, start, size, who):
+        width = ins[i].shape[1]
+        return outs[i].at[
+            pl.ds(start, size), pl.ds(pl.multiple_of(who * width, 128), width)
+        ]
+
+    started = []
+    for p, (i, start, size) in enumerate(pieces):
+        src = ins[i].at[pl.ds(start, size)]
+        for k in range(half - 1):
+            cp = remote(
+                src, spot(i, start, size, me), send_sem.at[1 + k, p], recv_sem.at[1 + k, p], "tp", onward[k]
+            )
+            cp.start()
+            started.append(cp)
+    for p, (i, start, size) in enumerate(pieces):
+        src = ins[i].at[pl.ds(start, size)]
+        cp = remote(src, spot(i, start, size, me), send_sem.at[0, p], recv_sem.at[0, p], "tp", sibling)
+        cp.start()
+        started.append(cp)
+    locals_ = []
+    for i in range(m):
+        cp = pltpu.make_async_copy(ins[i], spot(i, 0, ins[i].shape[0], me), local_sem.at[i])
+        cp.start()
+        locals_.append(cp)
+    for p, (i, start, size) in enumerate(pieces):
+        for k in range(half - 1):
+            here = spot(i, start, size, origin[k])
+            remote(here, here, send_sem.at[1 + k, p], recv_sem.at[1 + k, p], "tp", sibling).wait_recv()
+            cp = remote(here, here, send_sem.at[half + k, p], recv_sem.at[half + k, p], "tp", sibling)
+            cp.start()
+            started.append(cp)
+    for p, (i, start, size) in enumerate(pieces):
+        here = spot(i, start, size, sibling)
+        remote(here, here, send_sem.at[0, p], recv_sem.at[0, p], "tp", sibling).wait_recv()
+        for k in range(half - 1):
+            here = spot(i, start, size, theirs[k])
+            remote(here, here, send_sem.at[half + k, p], recv_sem.at[half + k, p], "tp", sibling).wait_recv()
+    for cp in started:
+        cp.wait_send()
+    for cp in locals_:
+        cp.wait()
+
+
+def gather_tp(arrays, counts, ident):
+    n = lax.axis_size("tp")
+    if not small_mesh():
+        return [lax.all_gather(a, "tp", axis=1, tiled=True) for a in arrays]
+    total = sum(counts)
+    return pl.pallas_call(
+        functools.partial(gather_kernel, n, counts),
+        out_shape=[jax.ShapeDtypeStruct((a.shape[0], a.shape[1] * n), a.dtype) for a in arrays],
+        in_specs=[pl.BlockSpec(memory_space=pltpu.VMEM)] * len(arrays),
+        out_specs=[pl.BlockSpec(memory_space=pl.ANY)] * len(arrays),
+        scratch_shapes=[
+            pltpu.SemaphoreType.DMA((n, total)),
+            pltpu.SemaphoreType.DMA((n, total)),
+            pltpu.SemaphoreType.DMA((len(arrays),)),
+        ],
+        compiler_params=pltpu.CompilerParams(collective_id=ident, has_side_effects=True),
+        name="gather_tp_%d" % ident,
+    )(*arrays)
+
+
+def swap_kernel(n, select, m, *refs):
+    ins, outs = refs[:m], refs[m : 2 * m]
+    send_sem, recv_sem, local_sem = refs[2 * m :]
+    me = lax.axis_index("sp")
+    peers = [(me + k) % n for k in range(1, n)]
+    greet(["sp"] * (n - 1), peers)
+    started = []
+    for k in sorted(range(1, n), key=lambda v: -min(v, n - v)):
+        for i in range(m):
+            row = (me + k) // n if select else peers[k - 1]
+            cp = remote(
+                ins[i].at[row], outs[i].at[me], send_sem.at[i, k], recv_sem.at[i, k], "sp", peers[k - 1]
+            )
+            cp.start()
+            started.append(cp)
+    locals_ = []
+    for i in range(m):
+        cp = pltpu.make_async_copy(ins[i].at[0 if select else me], outs[i].at[me], local_sem.at[i])
+        cp.start()
+        locals_.append(cp)
+    for k in range(1, n):
+        for i in range(m):
+            here = outs[i].at[(me + n - k) % n]
+            remote(here, here, send_sem.at[i, k], recv_sem.at[i, k], "sp", peers[k - 1]).wait_recv()
+    for cp in started:
+        cp.wait_send()
+    for cp in locals_:
+        cp.wait()
+
+
+def swap_sp(arrays, ident, select=False):
+    n = lax.axis_size("sp")
+    if not small_mesh():
+        if select:
+            later = jnp.arange(n) > lax.axis_index("sp")
+            arrays = [
+                jnp.where(later[:, None, None], a[0][None], a[1][None]) for a in arrays
+            ]
+        return [lax.all_to_all(a, "sp", split_axis=0, concat_axis=0, tiled=True) for a in arrays]
+    m = len(arrays)
+    return pl.pallas_call(
+        functools.partial(swap_kernel, n, select, m),
+        out_shape=[jax.ShapeDtypeStruct((n,) + a.shape[1:], a.dtype) for a in arrays],
+        in_specs=[pl.BlockSpec(memory_space=pltpu.VMEM)] * m,
+        out_specs=[pl.BlockSpec(memory_space=pl.ANY)] * m,
+        scratch_shapes=[
+            pltpu.SemaphoreType.DMA((m, n)),
+            pltpu.SemaphoreType.DMA((m, n)),
+            pltpu.SemaphoreType.DMA((m,)),
+        ],
+        compiler_params=pltpu.CompilerParams(collective_id=ident, has_side_effects=True),
+        name="swap_sp_%d" % ident,
+    )(*arrays)
+
+
+def dispatch_kernel(n, t, in_ref, out_ref, go_s, go_r, fan_s, fan_r, local_sem):
+    half = t // 2
+    width = in_ref.shape[2]
+    me, mine = lax.axis_index("sp"), lax.axis_index("tp")
+    row, core = mine // 2, mine % 2
+    sibling = row * 2 + 1 - core
+    onward = [((row + k) % half) * 2 + core for k in range(1, half)]
+    origin = [((row + half - k) % half) * 2 + core for k in range(1, half)]
+    theirs = [((row + half - k) % half) * 2 + 1 - core for k in range(1, half)]
+    peers = [(me + k) % n for k in range(1, n)]
+    greet(["sp"] * (n - 1) + ["tp"] * half, peers + [sibling] + onward)
+
+    def spot(source, who):
+        return out_ref.at[source, :, pl.ds(pl.multiple_of(who * width, 128), width)]
+
+    started = []
+    for k in sorted(range(1, n), key=lambda v: -min(v, n - v)):
+        cp = remote(in_ref.at[peers[k - 1]], spot(me, mine), go_s.at[k], go_r.at[k], "sp", peers[k - 1])
+        cp.start()
+        started.append(cp)
+    keep = pltpu.make_async_copy(in_ref.at[me], spot(me, mine), local_sem.at[0])
+    keep.start()
+
+    def fan(k, src, source):
+        for j in range(half - 1):
+            cp = remote(src, spot(source, mine), fan_s.at[1 + j, k], fan_r.at[1 + j, k], "tp", onward[j])
+            cp.start()
+            started.append(cp)
+        cp = remote(src, spot(source, mine), fan_s.at[0, k], fan_r.at[0, k], "tp", sibling)
+        cp.start()
+        started.append(cp)
+
+    def hand(k, source):
+        for j in range(half - 1):
+            here = spot(source, origin[j])
+            remote(here, here, fan_s.at[1 + j, k], fan_r.at[1 + j, k], "tp", sibling).wait_recv()
+            cp = remote(here, here, fan_s.at[half + j, k], fan_r.at[half + j, k], "tp", sibling)
+            cp.start()
+            started.append(cp)
+
+    fan(0, in_ref.at[me], me)
+    order = [0] + sorted(range(1, n), key=lambda v: (min(v, n - v), v))
+    source = [(me + n - k) % n for k in range(n)]
+    for at, k in enumerate(order):
+        if k:
+            here = spot(source[k], mine)
+            remote(here, here, go_s.at[k], go_r.at[k], "sp", peers[k - 1]).wait_recv()
+            fan(k, here, source[k])
+        if at >= 2:
+            hand(order[at - 2], source[order[at - 2]])
+    for k in order[-2:]:
+        hand(k, source[k])
+    for k in order:
+        here = spot(source[k], sibling)
+        remote(here, here, fan_s.at[0, k], fan_r.at[0, k], "tp", sibling).wait_recv()
+        for j in range(half - 1):
+            here = spot(source[k], theirs[j])
+            remote(here, here, fan_s.at[half + j, k], fan_r.at[half + j, k], "tp", sibling).wait_recv()
+    for cp in started:
+        cp.wait_send()
+    keep.wait()
+
+
+def dispatch(outgoing, ident):
+    n, t = lax.axis_size("sp"), lax.axis_size("tp")
+    if not small_mesh():
+        arrived = lax.all_to_all(outgoing, "sp", split_axis=0, concat_axis=0, tiled=True)
+        return lax.all_gather(arrived, "tp", axis=2, tiled=True)
+    return pl.pallas_call(
+        functools.partial(dispatch_kernel, n, t),
+        out_shape=jax.ShapeDtypeStruct(
+            outgoing.shape[:2] + (outgoing.shape[2] * t,), outgoing.dtype
+        ),
+        in_specs=[pl.BlockSpec(memory_space=pltpu.VMEM)],
+        out_specs=pl.BlockSpec(memory_space=pl.ANY),
+        scratch_shapes=[
+            pltpu.SemaphoreType.DMA((n,)),
+            pltpu.SemaphoreType.DMA((n,)),
+            pltpu.SemaphoreType.DMA((t, n)),
+            pltpu.SemaphoreType.DMA((t, n)),
+            pltpu.SemaphoreType.DMA((1,)),
+        ],
+        compiler_params=pltpu.CompilerParams(collective_id=ident, has_side_effects=True),
+        name="dispatch_%d" % ident,
+    )(outgoing)
 
 
 def shards(
@@ -85,16 +338,23 @@
         increment_logits.astype(jnp.float32) + increment_offset[:, None, :]
     )
     log_fade_amount = -jnp.exp(log_fade_speed)[:, None, :] * increment_lengths + extra_log_fade
-    forward_cum = jnp.cumsum(log_fade_amount[0], axis=0)
-    backward_cum = jnp.cumsum(log_fade_amount[1], axis=0) - log_fade_amount[1]
-    forward_total = forward_cum[-1]
-    backward_total = backward_cum[-1] + log_fade_amount[1][-1]
-    scores = lax.dot_general(
-        c_conv, b_conv, (((1,), (1,)), ((), ())), preferred_element_type=jnp.float32
-    )
     position = jnp.arange(length)
     lower = position[:, None] >= position[None, :]
     upper = position[:, None] <= position[None, :]
+    both = jnp.concatenate([log_fade_amount[0], log_fade_amount[1]], axis=1)
+    sums = jnp.dot(
+        lower.astype(jnp.float32),
+        both,
+        precision=lax.Precision.HIGHEST,
+        preferred_element_type=jnp.float32,
+    )
+    forward_cum = sums[:, :heads_here]
+    backward_cum = sums[:, heads_here:] - log_fade_amount[1]
+    forward_total = sums[-1, :heads_here]
+    backward_total = sums[-1, heads_here:]
+    scores = lax.dot_general(
+        c_conv, b_conv, (((1,), (1,)), ((), ())), preferred_element_type=jnp.float32
+    )
     forward_gap = forward_cum.T[:, :, None] - forward_cum.T[:, None, :]
     backward_gap = backward_cum.T[:, None, :] - backward_cum.T[:, :, None]
     forward_part = (
@@ -114,31 +374,29 @@
     ).astype(jnp.bfloat16)
     own_states = jnp.einsum("dshp,sn->dhpn", scaled, b_conv, preferred_element_type=jnp.float32)
     own_logs = jnp.stack([forward_total, backward_total])
-    logs_all, states_all = (
-        lax.all_gather(own_logs[None], "sp", axis=0, tiled=True),
-        lax.all_gather(own_states[None], "sp", axis=0, tiled=True),
-    )
+    blocks = lax.axis_size("sp")
     own_index = lax.axis_index("sp")
-    running = jnp.cumsum(logs_all, axis=0)
-    before = running - logs_all
-    running_own = lax.dynamic_index_in_dim(running, own_index, 0, keepdims=False)
-    before_own = lax.dynamic_index_in_dim(before, own_index, 0, keepdims=False)
-    block_index = jnp.arange(logs_all.shape[0])[:, None]
-    earlier = block_index < own_index
-    later = block_index > own_index
-    weight_forward = jnp.where(
-        earlier, jnp.exp(jnp.where(earlier, before_own[0][None, :] - running[:, 0], 0.0)), 0.0
-    )
-    weight_backward = jnp.where(
-        later, jnp.exp(jnp.where(later, before[:, 1] - running_own[1][None, :], 0.0)), 0.0
-    )
-    carried_forward = jnp.einsum(
-        "jh,jhpn->hpn", weight_forward, states_all[:, 0], precision=lax.Precision.HIGHEST
-    )
-    carried_backward = jnp.einsum(
-        "jh,jhpn->hpn", weight_backward, states_all[:, 1], precision=lax.Precision.HIGHEST
-    )
-    carried = jnp.stack([carried_forward, carried_backward]).astype(jnp.bfloat16)
+    states_all, logs_all = swap_sp(
+        [
+            own_states.astype(jnp.bfloat16).reshape(2, heads_here * head_size, STATE),
+            jnp.broadcast_to(own_logs[:, :, None], (2, heads_here, 128)),
+        ],
+        1,
+        True,
+    )
+    logs_all = logs_all[:, :, 0]
+    states_all = states_all.reshape(blocks, heads_here, head_size, STATE).astype(jnp.float32)
+    index = jnp.arange(blocks)
+    earlier = (index < own_index)[:, None]
+    later = (index > own_index)[:, None]
+    after = (index[None, :] > index[:, None])[:, :, None]
+    ahead = (index[None, :] < index[:, None])[:, :, None]
+    gap_forward = jnp.sum(jnp.where(after & earlier[None], logs_all[None], 0.0), axis=1)
+    gap_backward = jnp.sum(jnp.where(ahead & later[None], logs_all[None], 0.0), axis=1)
+    weight_forward = jnp.where(earlier, jnp.exp(jnp.where(earlier, gap_forward, 0.0)), 0.0)
+    weight_backward = jnp.where(later, jnp.exp(jnp.where(later, gap_backward, 0.0)), 0.0)
+    weights = jnp.stack([weight_forward, weight_backward])
+    carried = jnp.sum(weights[:, :, :, None, None] * states_all[None], axis=1).astype(jnp.bfloat16)
     readout = jnp.einsum("tn,dhpn->dthp", c_conv, carried, preferred_element_type=jnp.float32)
     mixer = (
         inner
@@ -149,67 +407,71 @@
     gated = mixer * jax.nn.silu(result_valve_logits.astype(jnp.float32)).reshape(
         length, heads_here, head_size
     )
-    squares = jnp.sum(gated * gated, axis=(1, 2))
-    group_marks = (jnp.arange(GROUPS) == group).astype(jnp.float32)
-    group_sums = lax.psum(squares[:, None] * group_marks[None, :], "tp")
-    own_sum = lax.dynamic_index_in_dim(group_sums, group, 1, keepdims=False)
+    own_sum = jnp.sum(gated * gated, axis=(1, 2))
+    if heads_here < spread:
+        group_marks = (jnp.arange(GROUPS) == group).astype(jnp.float32)
+        group_sums = lax.psum(own_sum[:, None] * group_marks[None, :], "tp")
+        own_sum = lax.dynamic_index_in_dim(group_sums, group, 1, keepdims=False)
     scale = lax.rsqrt(own_sum / (spread * HEAD_DIM) + 1e-06)
     normed = (
         gated.reshape(length, channels) * scale[:, None] * cluster_rescale_factor[None, :]
     ).astype(jnp.bfloat16)
-    projected = jnp.dot(
-        lax.all_gather(normed, "tp", axis=1, tiled=True),
-        blender_result_matrix,
-        preferred_element_type=jnp.float32,
-    )
+    normed_all, rescale_all = gather_tp(
+        [normed, specialist_rescale_factor[None, :]], (1, 1), 2
+    )
+    projected = jnp.dot(normed_all, blender_result_matrix, preferred_element_type=jnp.float32)
     after_mixer = (layer_source_vector.astype(jnp.float32) + projected).astype(jnp.bfloat16)
     resid = after_mixer.astype(jnp.float32)
-    total_squares = lax.psum(jnp.sum(resid * resid, axis=1), "tp")
-    features = (
-        resid * lax.rsqrt(total_squares / D + 1e-06)[:, None] * specialist_rescale_factor[None, :]
-    ).astype(jnp.bfloat16)
-    full_features = lax.all_gather(features, "tp", axis=1, tiled=True)
+    (after_all,) = gather_tp([after_mixer], (2,), 3)
+    resid_all = after_all.astype(jnp.float32)
+    inverse = lax.rsqrt(jnp.sum(resid_all * resid_all, axis=1) / D + 1e-06)[:, None]
+    full_features = (resid_all * inverse * rescale_all).astype(jnp.bfloat16)
+    features = (resid * inverse * specialist_rescale_factor[None, :]).astype(jnp.bfloat16)
+    top = chosen_specialists.shape[1]
+    experts = lax.axis_size("sp")
+    capacity = 3 * length * top // (2 * experts)
+    marks = (
+        chosen_specialists[:, :, None] == jnp.arange(experts, dtype=jnp.int32)[None, None, :]
+    ).astype(jnp.float32)
+    strict = (position[:, None] > position[None, :]).astype(jnp.bfloat16)
+    earlier_rows = jnp.dot(
+        strict, jnp.sum(marks, axis=1).astype(jnp.bfloat16), preferred_element_type=jnp.float32
+    )
+    rank = jnp.sum(earlier_rows[:, None, :] * marks, axis=2).astype(jnp.int32)
+    slot = chosen_specialists * capacity + rank
+    slots = jnp.arange(experts * capacity, dtype=jnp.int32)
+    pick = sum((slots[:, None] == slot[None, :, j]).astype(jnp.bfloat16) for j in range(top))
+    outgoing = jnp.dot(pick, features, preferred_element_type=jnp.float32).astype(jnp.bfloat16)
+    arrived = dispatch(outgoing.reshape(experts, capacity, -1), 4)
+    arrived = arrived.reshape(experts * capacity, -1)
     shared_hidden = (
         jax.nn.silu(jnp.dot(full_features, common_valve_matrix, preferred_element_type=jnp.float32))
         * jnp.dot(full_features, common_raising_matrix, preferred_element_type=jnp.float32)
     ).astype(jnp.bfloat16)
-    top = chosen_specialists.shape[1]
-    experts = lax.axis_size("sp")
-    capacity = 3 * length * top // (2 * experts)
-    flat = chosen_specialists.reshape(-1)
-    one_hot = (flat[:, None] == jnp.arange(experts, dtype=jnp.int32)[None, :]).astype(jnp.int32)
-    rank = jnp.sum((jnp.cumsum(one_hot, axis=0) - one_hot) * one_hot, axis=1)
-    slot = flat * capacity + rank
-    token = jnp.arange(length * top, dtype=jnp.int32) // top
-    owner = jnp.zeros((experts * capacity,), jnp.int32).at[slot].set(token)
-    filled = jnp.zeros((experts * capacity,), jnp.bool_).at[slot].set(True)
-    outgoing = jnp.where(
-        filled[:, None], jnp.take(full_features, owner, axis=0), jnp.zeros((), jnp.bfloat16)
-    ).reshape(experts, capacity, -1)
-    arrived = lax.all_to_all(outgoing, "sp", split_axis=0, concat_axis=0, tiled=True)
-    arrived = arrived.reshape(-1, arrived.shape[2])
     expert_hidden = (
         jax.nn.silu(
             jnp.dot(arrived, specialist_valve_matrix[0], preferred_element_type=jnp.float32)
         )
         * jnp.dot(arrived, specialist_raising_matrix[0], preferred_element_type=jnp.float32)
     ).astype(jnp.bfloat16)
-    expert_all, shared_all = (
-        lax.all_gather(expert_hidden, "tp", axis=1, tiled=True),
-        lax.all_gather(shared_hidden, "tp", axis=1, tiled=True),
-    )
+    expert_all, shared_all = gather_tp([expert_hidden, shared_hidden], (4, 2), 5)
     expert_out = jnp.dot(
         expert_all, specialist_lowering_matrix[0], preferred_element_type=jnp.float32
     ).astype(jnp.bfloat16)
     shared_out = jnp.dot(
         shared_all, common_lowering_matrix, preferred_element_type=jnp.float32
     ).astype(jnp.bfloat16)
-    returned = lax.all_to_all(
-        expert_out.reshape(experts, capacity, -1), "sp", split_axis=0, concat_axis=0, tiled=True
-    )
-    picked = jnp.take(returned.reshape(experts * capacity, -1), slot, axis=0).astype(jnp.float32)
-    picked = picked.reshape(length, top, -1)
-    routed = jnp.sum(picked * specialist_shares[:, :, None], axis=1)
+    (returned,) = swap_sp([expert_out.reshape(experts, capacity, -1)], 6)
+    returned = returned.reshape(experts * capacity, -1)
+    shares = sum(
+        jnp.where(slots[None, :] == slot[:, j, None], specialist_shares[:, j, None], 0.0)
+        for j in range(top)
+    )
+    high = shares.astype(jnp.bfloat16)
+    low = (shares - high.astype(jnp.float32)).astype(jnp.bfloat16)
+    routed = jnp.dot(high, returned, preferred_element_type=jnp.float32) + jnp.dot(
+        low, returned, preferred_element_type=jnp.float32
+    )
     return (resid + shared_out.astype(jnp.float32) + routed).astype(jnp.bfloat16)
 
 

time: 325 us -> 207 us (0.64)
  Pallas kernels: 0 us -> 147 us
  blocking collectives: 136 us -> 0 us
  waiting for transfers between devices: 81.2 us -> 0.01 us
  local copies, waits for them, and re-layouts: 28.9 us -> 7.81 us
  between operations: 13.7 us -> 0.51 us
  other arithmetic: 22 us -> 13.4 us
  starting transfers between devices: 12 us -> 6.17 us
    pallas_call x0 -> x6, Pallas kernels: none -> 147 us  [the longest x3 55.9 us: gather_tp(): pl.pallas_call(functools.partial(gather_kernel, n, counts), out_shape=[ja...]
    all_to_all x1 -> x0, blocking collectives: 93.2 us -> none  [shards(): lax.all_to_all(outgoing, 'sp', split_axis=0, concat_axis=0, tiled=True)]
    all_gather x4 -> x0, waiting for transfers between devices: 61.2 us -> none  [the longest x1 28 us: shards(): lax.all_gather(expert_hidden, 'tp', axis=1, tiled=True)]
    all_gather x2 -> x0, blocking collectives: 30.8 us -> none  [the longest x1 22 us: shards(): lax.all_gather(own_logs[None], 'sp', axis=0, tiled=True)]
    all_to_all x1 -> x0, waiting for transfers between devices: 20 us -> none  [shards(): lax.all_to_all(expert_out.reshape(experts, capacity, -1), 'sp', split_axi...]
    gather x3 -> x0, local copies, waits for them, and re-layouts: 14.6 us -> none  [the longest x1 10.2 us: shards(): jnp.take(full_features, owner, axis=0)]
    psum x2 -> x0, blocking collectives: 12.1 us -> none  [the longest x1 6.4 us: shards(): total_squares = lax.psum(jnp.sum(resid * resid, axis=1), 'tp')]
    scatter x2 -> x0, local copies, waits for them, and re-layouts: 7.18 us -> none  [the longest x1 4.28 us: shards(): owner = jnp.zeros((experts * capacity,), jnp.int32).at[slot].set(token)]
  transfers between devices with their start and end apart: 7 -> 2, of which waited for: 4 -> 0; matrix products, arithmetic and copies ran while one was open for 12% -> 5% of each run, Pallas kernels for 0% -> 0%
where the time goes in v1:
time: 207 us; the launch traced here: 205 us
  Pallas kernels  147 us (71%)
  matrix products  30.3 us (15%)
  other arithmetic  13.4 us (6%)
  local copies, waits for them, and re-layouts  7.81 us (4%)
  starting transfers between devices  6.17 us (3%)
    pallas_call x3, Pallas kernels, gather_tp(): pl.pallas_call(functools.partial(gather_kernel, n, counts), out_shape=[ja...  55.9 us
    pallas_call x1, Pallas kernels, dispatch(): pl.pallas_call(functools.partial(dispatch_kernel, n, t), out_shape=jax.Sh...  47.1 us
    pallas_call x2, Pallas kernels, swap_sp(): pl.pallas_call(functools.partial(swap_kernel, n, select, m), out_shape=[j...  43.8 us
    dot_general x1, matrix products, shards(): jnp.dot(expert_all, specialist_lowering_matrix[0], preferred_element_type...  6.15 us
    ppermute x1, starting transfers between devices, extended(): lax.ppermute(tail, axis, [(i, (i + 1) % count) for i in range(ends)])  4.88 us
  transfers between devices with their start and end apart: 2, of which 0 were waited for; matrix products, arithmetic and copies ran while one was open for 5% of the time, Pallas kernels for 0%

profile of v1, /device:TPU:0, one launch (start us, length us, event | category | flops | bytes accessed | tf_op | source)
XLA Modules:
  0.0 205.1 jit_solution(6941628749770239853)
XLA Ops:
  0.0 1.1 constant_dynamic-slice_fusion.2
  1.1 0.9 pad_maximum_fusion.1
  2.1 4.9 %collective-permute-start = (bf16[2,512]{1,0:T(2,128)(2,1)S(1)}, bf16[2,512]{1,0:T(2,128)(2,1)S(1)}, u32[]{:S(2)}, u32[]{:S(2)}) collective-permute-start(bf16[2,512]{1,0:T(2,128)(2,1)S(1)} %get-tuple-element.27), channel_id=1, source_target_pairs={{0,4},{4,8},{8,12},{12,16},{16,20},{20,24},{24,28},{1,5},{5,9},{9,... | collective-permute-start | bytes 6152 | tf_op jit(solution)/shard_map/ppermute | solution.py:29
  7.0 1.3 collective-permute-start.1
  8.3 0.8 iota_compare_fusion.5
  9.1 0.7 constant_dynamic-slice_fusion
  11.2 0.8 multiply_add_fusion
  13.7 1.0 convert_multiply_fusion.3
  17.0 0.9 copy.48
  19.0 0.9 convolution_convert_fusion.2
  20.6 17.3 %swap_sp_1.1 = (bf16[8,256,128]{2,1,0:T(8,128)(2,1)}, f32[8,4,128]{2,1,0:T(4,128)}) custom-call(bf16[2,256,128]{2,1,0:T(8,128)(2,1)} %bitcast.135, f32[2,4,128]{2,1,0:T(4,128)} %broadcast_in_dim.159.refs_1_), custom_call_target="tpu_custom_call" | custom-call | tf_op jit(solution)/shard_map/swap_sp_1/pallas_call | solution.py:182
  37.9 0.8 copy.46
  38.7 0.8 select_reduce_fusion.2
  40.8 1.2 bitcast_convert_fusion
  42.5 3.1 %multiply_reduce_fusion.1 = (f32[320]{0:T(512)S(1)}, f32[320,4,64]{0,2,1:T(8,128)}) fusion(f32[320,4,64]{0,2,1:T(8,128)S(1)} %bitcast.136, bf16[320,4,64]{0,2,1:T(8,128)(2,1)S(1)} %bitcast.134, f32[4]{0:T(128)S(1)} %copy-done.24, f32[2,320,4,64]{1,3,2,0:T(8,128)S(1)} %convolution_bitcast_fusion, f32[320,4]{0,1:T(4,128)S(1)} %get-tuple-element.29, ...), kind=kOutput, calls=%fused_computation.75 | convolution fusion | flops 57753280 | bytes 2688768 | tf_op jit(solution)/shard_map/hts,shp->thp/dot_general | solution.py:369
  45.7 1.1 copy.49
  46.8 0.8 multiply_convert_fusion.6.refs_0_
  47.6 9.0 %gather_tp_2.1 = (bf16[320,1024]{1,0:T(8,128)(2,1)}, f32[1,2048]{1,0:T(1,128)}) custom-call(bf16[320,256]{1,0:T(8,128)(2,1)} %multiply_convert_fusion.6.refs_0_, f32[1,512]{1,0:T(1,128)} %bitcast.145), custom_call_target="tpu_custom_call" | custom-call | tf_op jit(solution)/shard_map/gather_tp_2/pallas_call | solution.py:127
  56.6 2.7 %fusion.18.refs_0_ = bf16[320,512]{1,0:T(8,128)(2,1)} fusion(bf16[320,1024]{1,0:T(8,128)(2,1)} %get-tuple-element.13, bf16[1024,512]{1,0:T(8,128)(2,1)} %param.38, bf16[320,512]{1,0:T(8,128)(2,1)S(1)} %copy-done.22), kind=kOutput, calls=%fused_computation.30 | convolution fusion | flops 336035840 | bytes 2359296 | tf_op jit(solution)/shard_map/dot_general | solution.py:422
  59.3 12.7 %gather_tp_3.1 = bf16[320,2048]{1,0:T(8,128)(2,1)} custom-call(bf16[320,512]{1,0:T(8,128)(2,1)} %fusion.18.refs_0_), custom_call_target="tpu_custom_call" | custom-call | tf_op jit(solution)/shard_map/gather_tp_3/pallas_call | solution.py:127
  71.9 1.7 fusion
  73.6 1.8 convolution_convert_fusion
  75.4 47.1 %dispatch_4.1 = bf16[8,120,2048]{2,1,0:T(8,128)(2,1)} custom-call(bf16[8,120,512]{2,1,0:T(8,128)(2,1)} %bitcast.130), custom_call_target="tpu_custom_call" | custom-call | tf_op jit(solution)/shard_map/dispatch_4/pallas_call | solution.py:265
  122.6 2.6 %fusion.57 = f32[320,512]{1,0:T(8,128)S(1)} fusion(bf16[2048,512]{1,0:T(8,128)(2,1)} %param.45, bf16[320,2048]{1,0:T(8,128)(2,1)S(1)} %copy-done.1, f32[2048]{0:T(1024)S(1)} %bitcast.146, f32[320]{0:T(512)S(1)} %add_rsqrt_fusion), kind=kOutput, calls=%fused_computation.78 | convolution fusion | flops 673710080 | bytes 4072704 | tf_op jit(solution)/shard_map/dot_general | solution.py:448
  125.2 1.7 fusion.19.refs_1_
  127.5 2.2 %fusion.7 = f32[960,512]{1,0:T(8,128)S(1)} fusion(bf16[960,2048]{1,0:T(8,128)(2,1)S(1)} %bitcast.128, bf16[1,2048,512]{2,1,0:T(8,128)(2,1)S(1)} %copy-done), kind=kOutput, calls=%fused_computation.9 | convolution fusion | flops 2013265920 | bytes 7995392 | tf_op jit(solution)/shard_map/dot_general | solution.py:453
  129.6 3.4 %multiply_convert_fusion.refs_0_ = bf16[960,512]{1,0:T(8,128)(2,1)} fusion(f32[960,512]{1,0:T(8,128)S(1)} %fusion.7, bf16[960,2048]{1,0:T(8,128)(2,1)S(1)} %bitcast.129, bf16[1,2048,512]{2,1,0:T(8,128)(2,1)S(1)} %copy-done.21), kind=kOutput, calls=%fused_computation.12 | convolution fusion | flops 2016215040 | bytes 8978432 | tf_op jit(solution)/shard_map/dot_general | solution.py:455
  133.0 34.3 %gather_tp_5.1 = (bf16[960,2048]{1,0:T(8,128)(2,1)}, bf16[320,2048]{1,0:T(8,128)(2,1)}) custom-call(bf16[960,512]{1,0:T(8,128)(2,1)} %multiply_convert_fusion.refs_0_, bf16[320,512]{1,0:T(8,128)(2,1)} %fusion.19.refs_1_), custom_call_target="tpu_custom_call" | custom-call | tf_op jit(solution)/shard_map/gather_tp_5/pallas_call | solution.py:127
  167.3 6.1 %fusion.13 = bf16[960,512]{1,0:T(8,128)(2,1)} fusion(bf16[960,2048]{1,0:T(8,128)(2,1)} %get-tuple-element.16, bf16[1,2048,512]{2,1,0:T(8,128)(2,1)} %param.44), kind=kOutput, calls=%fused_computation.19 | convolution fusion | flops 2013757440 | bytes 7012352 | tf_op jit(solution)/shard_map/dot_general | solution.py:458
  173.5 26.6 %swap_sp_6.1 = bf16[8,120,512]{2,1,0:T(8,128)(2,1)} custom-call(bf16[8,120,512]{2,1,0:T(8,128)(2,1)} %bitcast.133), custom_call_target="tpu_custom_call" | custom-call | tf_op jit(solution)/shard_map/swap_sp_6/pallas_call | solution.py:182
  200.1 2.9 %fusion.22 = f32[320,512]{1,0:T(8,128)S(1)} fusion(bf16[320,2048]{1,0:T(8,128)(2,1)} %get-tuple-element.15, bf16[2048,512]{1,0:T(8,128)(2,1)} %param.47, bf16[320,512]{1,0:T(8,128)(2,1)S(1)} %copy-done.7), kind=kOutput, calls=%fused_computation.35 | convolution fusion | flops 671744000 | bytes 4390912 | tf_op jit(solution)/shard_map/dot_general | solution.py:461
  203.7 1.4 fusion.20
  (88 shorter events, 10.0 us)
Async XLA Ops:
  0.0 126.9 %copy-start = (bf16[1,2048,512]{2,1,0:T(8,128)(2,1)S(1)}, bf16[1,2048,512]{2,1,0:T(8,128)(2,1)}, u32[]{:S(2)}) copy-start(bf16[1,2048,512]{2,1,0:T(8,128)(2,1)} %param.42) | copy-start | bytes 6291460
  0.0 17.9 %copy-start.3 = (bf16[320,256]{1,0:T(8,128)(2,1)S(1)}, bf16[320,256]{1,0:T(8,128)(2,1)}, u32[]{:S(2)}) copy-start(bf16[320,256]{1,0:T(8,128)(2,1)} %param.25) | copy-start | bytes 491524
  0.0 14.7 %copy-start.10 = (s32[320,2]{0,1:T(2,128)S(1)}, s32[320,2]{0,1:T(2,128)}, u32[]{:S(2)}) copy-start(s32[320,2]{0,1:T(2,128)} %param.40) | copy-start | bytes 7684
  0.0 15.6 %copy-start.11 = (f32[320,2]{0,1:T(2,128)S(1)}, f32[320,2]{0,1:T(2,128)}, u32[]{:S(2)}) copy-start(f32[320,2]{0,1:T(2,128)} %param.41) | copy-start | bytes 7684
  2.1 15.8 %collective-permute-start = (bf16[2,512]{1,0:T(2,128)(2,1)S(1)}, bf16[2,512]{1,0:T(2,128)(2,1)S(1)}, u32[]{:S(2)}, u32[]{:S(2)}) collective-permute-start(bf16[2,512]{1,0:T(2,128)(2,1)S(1)} %get-tuple-element.27), channel_id=1, source_target_pairs={{0,4},{4,8},{8,12},{12,16},{16,20},{20,24},{24,28},{1,5},{5,9},{9,... | collective-permute-start | bytes 6152 | tf_op jit(solution)/shard_map/ppermute | solution.py:29
  7.0 10.9 %collective-permute-start.1 = (bf16[2,512]{1,0:T(2,128)(2,1)S(1)}, bf16[2,512]{1,0:T(2,128)(2,1)S(1)}, u32[]{:S(2)}, u32[]{:S(2)}) collective-permute-start(bf16[2,512]{1,0:T(2,128)(2,1)S(1)} %get-tuple-element.28), channel_id=1, source_target_pairs={{4,0},{8,4},{12,8},{16,12},{20,16},{24,20},{28,24},{5,1},{9,5},{13... | collective-permute-start | bytes 6152 | tf_op jit(solution)/shard_map/ppermute | solution.py:31
  12.5 1.1 copy-start.18
  12.5 1.1 copy-start.19
  20.6 21.9 %copy-start.5 = (f32[320,256]{0,1:T(8,128)S(1)}, f32[320,256]{0,1:T(8,128)}, u32[]{:S(2)}) copy-start(f32[320,256]{0,1:T(8,128)} %copy.48) | copy-start | bytes 983044
  20.6 21.9 %copy-start.24 = (f32[4]{0:T(128)S(1)}, f32[4]{0:T(128)}, u32[]{:S(2)}) copy-start(f32[4]{0:T(128)} %param.33) | copy-start | bytes 52
  40.8 1.7 copy-start.8
  40.8 1.7 copy-start.9
  42.5 4.3 %copy-start.17 = (f32[256]{0:T(256)S(1)}, f32[256]{0:T(256)}, u32[]{:S(2)}) copy-start(f32[256]{0:T(256)} %param.37) | copy-start | bytes 3076
  42.5 14.1 %copy-start.22 = (bf16[320,512]{1,0:T(8,128)(2,1)S(1)}, bf16[320,512]{1,0:T(8,128)(2,1)}, u32[]{:S(2)}) copy-start(bf16[320,512]{1,0:T(8,128)(2,1)} %param.24) | copy-start | bytes 983044
  59.3 14.4 %copy-start.6 = (bf16[320,512]{1,0:T(8,128)(2,1)S(1)}, bf16[320,512]{1,0:T(8,128)(2,1)}, u32[]{:S(2)}) copy-start(bf16[320,512]{1,0:T(8,128)(2,1)} %fusion.18.refs_0_) | copy-start | bytes 983044
  59.3 14.4 %copy-start.12 = (s32[320]{0:T(512)S(1)}, s32[320]{0:T(512)}, u32[]{:S(2)}) copy-start(s32[320]{0:T(512)} %get-tuple-element.21) | copy-start | bytes 3844
  59.3 14.4 %copy-start.13 = (s32[320]{0:T(512)S(1)}, s32[320]{0:T(512)}, u32[]{:S(2)}) copy-start(s32[320]{0:T(512)} %get-tuple-element.22) | copy-start | bytes 3844
  59.3 14.4 %copy-start.16 = (f32[512]{0:T(512)S(1)}, f32[512]{0:T(512)}, u32[]{:S(2)}) copy-start(f32[512]{0:T(512)} %param.39) | copy-start | bytes 6148
  75.4 47.1 %copy-start.1 = (bf16[320,2048]{1,0:T(8,128)(2,1)S(1)}, bf16[320,2048]{1,0:T(8,128)(2,1)}, u32[]{:S(2)}) copy-start(bf16[320,2048]{1,0:T(8,128)(2,1)} %gather_tp_3.1) | copy-start | bytes 3932164
  75.4 47.1 %copy-start.23 = (f32[1,2048]{1,0:T(1,128)S(1)}, f32[1,2048]{1,0:T(1,128)}, u32[]{:S(2)}) copy-start(f32[1,2048]{1,0:T(1,128)} %get-tuple-element.14) | copy-start | bytes 24580
  122.6 2.6 %copy-start.20 = (bf16[2048,512]{1,0:T(8,128)(2,1)S(1)}, bf16[2048,512]{1,0:T(8,128)(2,1)}, u32[]{:S(2)}) copy-start(bf16[2048,512]{1,0:T(8,128)(2,1)} %param.46) | copy-start | bytes 6291460
  125.2 2.2 %copy-start.2 = (bf16[8,120,2048]{2,1,0:T(8,128)(2,1)S(1)}, bf16[8,120,2048]{2,1,0:T(8,128)(2,1)}, u32[]{:S(2)}) copy-start(bf16[8,120,2048]{2,1,0:T(8,128)(2,1)} %dispatch_4.1) | copy-start | bytes 11796484
  127.4 2.2 %copy-start.21 = (bf16[1,2048,512]{2,1,0:T(8,128)(2,1)S(1)}, bf16[1,2048,512]{2,1,0:T(8,128)(2,1)}, u32[]{:S(2)}) copy-start(bf16[1,2048,512]{2,1,0:T(8,128)(2,1)} %param.43) | copy-start | bytes 6291460
  173.5 26.6 %copy-start.7 = (bf16[320,512]{1,0:T(8,128)(2,1)S(1)}, bf16[320,512]{1,0:T(8,128)(2,1)}, u32[]{:S(2)}) copy-start(bf16[320,512]{1,0:T(8,128)(2,1)} %fusion.18.refs_0_) | copy-start | bytes 983044
  200.1 2.9 %copy-start.4 = (bf16[8,120,512]{2,1,0:T(8,128)(2,1)S(1)}, bf16[8,120,512]{2,1,0:T(8,128)(2,1)}, u32[]{:S(2)}) copy-start(bf16[8,120,512]{2,1,0:T(8,128)(2,1)} %swap_sp_6.1) | copy-start | bytes 2949124
  200.1 2.9 %copy-start.14 = (f32[320]{0:T(512)S(1)}, f32[320]{0:T(512)}, u32[]{:S(2)}) copy-start(f32[320]{0:T(512)} %get-tuple-element.19) | copy-start | bytes 3844
  200.1 2.9 %copy-start.15 = (f32[320]{0:T(512)S(1)}, f32[320]{0:T(512)}, u32[]{:S(2)}) copy-start(f32[320]{0:T(512)} %get-tuple-element.20) | copy-start | bytes 3844

commit v2 on v1

--- a/solution.py
+++ b/solution.py
@@ -194,91 +194,223 @@
     )(*arrays)
 
 
-def dispatch_kernel(n, t, in_ref, out_ref, go_s, go_r, fan_s, fan_r, local_sem):
+def dispatch(outgoing):
+    arrived = lax.all_to_all(outgoing, "sp", split_axis=0, concat_axis=0, tiled=True)
+    return lax.all_gather(arrived, "tp", axis=2, tiled=True)
+
+
+def experts_kernel(n, t, out_blk, feats, wg_ref, wu_ref, wl_ref, sg_ref, su_ref, sl_ref, ret, sout,
+                   arr, hid, hall, shid, sall, eout, wg, wu, wl, sg, su, sl,
+                   put_s, put_r, fan_s, fan_r, hid_s, hid_r, go_s, go_r, loc):
     half = t // 2
-    width = in_ref.shape[2]
     me, mine = lax.axis_index("sp"), lax.axis_index("tp")
     row, core = mine // 2, mine % 2
     sibling = row * 2 + 1 - core
     onward = [((row + k) % half) * 2 + core for k in range(1, half)]
     origin = [((row + half - k) % half) * 2 + core for k in range(1, half)]
     theirs = [((row + half - k) % half) * 2 + 1 - core for k in range(1, half)]
-    peers = [(me + k) % n for k in range(1, n)]
-    greet(["sp"] * (n - 1) + ["tp"] * half, peers + [sibling] + onward)
-
-    def spot(source, who):
-        return out_ref.at[source, :, pl.ds(pl.multiple_of(who * width, 128), width)]
-
+    peers = [(me + k) % n for k in range(n)]
+    source = [(me + n - k) % n for k in range(n)]
+    fetch = [
+        pltpu.make_async_copy(a, b, loc.at[i])
+        for i, (a, b) in enumerate(
+            ((sg_ref, sg), (su_ref, su), (wg_ref, wg), (wu_ref, wu), (wl_ref, wl), (sl_ref, sl))
+        )
+    ]
+    for cp in fetch:
+        cp.start()
+    greet(["sp"] * (n - 1) + ["tp"] * half, peers[1:] + [sibling] + onward)
     started = []
-    for k in sorted(range(1, n), key=lambda v: -min(v, n - v)):
-        cp = remote(in_ref.at[peers[k - 1]], spot(me, mine), go_s.at[k], go_r.at[k], "sp", peers[k - 1])
-        cp.start()
-        started.append(cp)
-    keep = pltpu.make_async_copy(in_ref.at[me], spot(me, mine), local_sem.at[0])
-    keep.start()
-
-    def fan(k, src, source):
+
+    def columns(who, width):
+        return pl.ds(pl.multiple_of(who * width, 128), width)
+
+    def first(k, who):
+        return arr.at[source[k], :, columns(who, out_blk.shape[2])]
+
+    def second(k, who):
+        if k == n:
+            return sall.at[:, columns(who, shid.shape[1])]
+        return hall.at[source[k], :, columns(who, hid.shape[2])]
+
+    def fan(src, spot, ss, rr, k):
         for j in range(half - 1):
-            cp = remote(src, spot(source, mine), fan_s.at[1 + j, k], fan_r.at[1 + j, k], "tp", onward[j])
+            cp = remote(src, spot(k, mine), ss.at[1 + j, k], rr.at[1 + j, k], "tp", onward[j])
             cp.start()
             started.append(cp)
-        cp = remote(src, spot(source, mine), fan_s.at[0, k], fan_r.at[0, k], "tp", sibling)
+        cp = remote(src, spot(k, mine), ss.at[0, k], rr.at[0, k], "tp", sibling)
         cp.start()
         started.append(cp)
 
-    def hand(k, source):
+    def hand(spot, ss, rr, k):
         for j in range(half - 1):
-            here = spot(source, origin[j])
-            remote(here, here, fan_s.at[1 + j, k], fan_r.at[1 + j, k], "tp", sibling).wait_recv()
-            cp = remote(here, here, fan_s.at[half + j, k], fan_r.at[half + j, k], "tp", sibling)
+            here = spot(k, origin[j])
+            remote(here, here, ss.at[1 + j, k], rr.at[1 + j, k], "tp", sibling).wait_recv()
+            cp = remote(here, here, ss.at[half + j, k], rr.at[half + j, k], "tp", sibling)
             cp.start()
             started.append(cp)
 
-    fan(0, in_ref.at[me], me)
-    order = [0] + sorted(range(1, n), key=lambda v: (min(v, n - v), v))
-    source = [(me + n - k) % n for k in range(n)]
-    for at, k in enumerate(order):
-        if k:
-            here = spot(source[k], mine)
-            remote(here, here, go_s.at[k], go_r.at[k], "sp", peers[k - 1]).wait_recv()
-            fan(k, here, source[k])
-        if at >= 2:
-            hand(order[at - 2], source[order[at - 2]])
-    for k in order[-2:]:
-        hand(k, source[k])
-    for k in order:
-        here = spot(source[k], sibling)
-        remote(here, here, fan_s.at[0, k], fan_r.at[0, k], "tp", sibling).wait_recv()
+    def landed(spot, ss, rr, k):
+        here = spot(k, sibling)
+        remote(here, here, ss.at[0, k], rr.at[0, k], "tp", sibling).wait_recv()
         for j in range(half - 1):
-            here = spot(source[k], theirs[j])
-            remote(here, here, fan_s.at[half + j, k], fan_r.at[half + j, k], "tp", sibling).wait_recv()
+            here = spot(k, theirs[j])
+            remote(here, here, ss.at[half + j, k], rr.at[half + j, k], "tp", sibling).wait_recv()
+
+    def product(rows, gate, up):
+        g = jnp.dot(rows, gate[...], preferred_element_type=jnp.float32)
+        return (jax.nn.silu(g) * jnp.dot(rows, up[...], preferred_element_type=jnp.float32)).astype(
+            jnp.bfloat16
+        )
+
+    far = sorted(range(1, n), key=lambda v: min(v, n - v))
+    order = [0] + far
+    for k in far:
+        cp = remote(out_blk.at[peers[k]], arr.at[me, :, columns(mine, out_blk.shape[2])],
+                    put_s.at[k], put_r.at[k], "sp", peers[k])
+        cp.start()
+        started.append(cp)
+    keep = pltpu.make_async_copy(out_blk.at[me], first(0, mine), loc.at[6])
+    keep.start()
+    locals_ = [keep]
+
+    def arrive(k):
+        if k == 0:
+            fan(out_blk.at[me], first, fan_s, fan_r, 0)
+            return
+        here = first(k, mine)
+        remote(here, here, put_s.at[k], put_r.at[k], "sp", peers[k]).wait_recv()
+        fan(here, first, fan_s, fan_r, k)
+
+    def spread(k):
+        src = shid if k == n else hid.at[source[k]]
+        fan(src, second, hid_s, hid_r, k)
+        cp = pltpu.make_async_copy(src, second(k, mine), loc.at[7 + k])
+        cp.start()
+        locals_.append(cp)
+        return cp
+
+    own = {}
+
+    def hidden(k):
+        landed(first, fan_s, fan_r, k)
+        if k == 0:
+            keep.wait()
+            fetch[2].wait()
+            fetch[3].wait()
+        hid[source[k]] = product(arr[source[k]], wg, wu)
+
+    def lowering(k):
+        landed(second, hid_s, hid_r, k)
+        own[k].wait()
+        if k == 0:
+            fetch[4].wait()
+        eout[source[k]] = jnp.dot(
+            hall[source[k]], wl[...], preferred_element_type=jnp.float32
+        ).astype(eout.dtype)
+
+    def give(k):
+        src = eout.at[source[k]]
+        if k == 0:
+            cp = pltpu.make_async_copy(src, ret.at[me], loc.at[8 + n])
+            cp.start()
+            own[-1] = cp
+            return
+        cp = remote(src, ret.at[me], go_s.at[k], go_r.at[k], "sp", source[k])
+        cp.start()
+        started.append(cp)
+
+    lag = 4
+    for s in range(n + lag):
+        if s < n:
+            arrive(order[s])
+        if s == 0:
+            fetch[0].wait()
+            fetch[1].wait()
+            shid[...] = product(feats[...], sg, su)
+        if s == 1:
+            own[n] = spread(n)
+        if 3 <= s <= lag:
+            own[order[s - 3]] = spread(order[s - 3])
+        if s == 3:
+            hand(second, hid_s, hid_r, n)
+        if 1 <= s <= n:
+            hand(first, fan_s, fan_r, order[s - 1])
+        if lag <= s < n + lag:
+            hand(second, hid_s, hid_r, order[s - lag])
+        if 2 <= s < n + 2:
+            hidden(order[s - 2])
+        if lag + 1 <= s < n + lag:
+            give(order[s - lag - 1])
+        if lag <= s < n + lag:
+            lowering(order[s - lag])
+        if lag <= s < n + 2:
+            own[order[s - 2]] = spread(order[s - 2])
+    landed(second, hid_s, hid_r, n)
+    own[n].wait()
+    fetch[5].wait()
+    sout[...] = jnp.dot(sall[...], sl[...], preferred_element_type=jnp.float32).astype(sout.dtype)
+    give(order[n - 1])
+    for k in far:
+        here = ret.at[peers[k]]
+        remote(here, here, go_s.at[k], go_r.at[k], "sp", source[k]).wait_recv()
     for cp in started:
         cp.wait_send()
-    keep.wait()
-
-
-def dispatch(outgoing, ident):
+    own[-1].wait()
+
+
+def all_experts(outgoing, features, weights, ident):
     n, t = lax.axis_size("sp"), lax.axis_size("tp")
-    if not small_mesh():
-        arrived = lax.all_to_all(outgoing, "sp", split_axis=0, concat_axis=0, tiled=True)
-        return lax.all_gather(arrived, "tp", axis=2, tiled=True)
+    blocks, slots, columns = outgoing.shape
+    length = features.shape[0]
+    units, out = weights[0].shape[1], weights[2].shape[1]
+    vmem, anywhere = pl.BlockSpec(memory_space=pltpu.VMEM), pl.BlockSpec(memory_space=pl.ANY)
+    half = jnp.bfloat16
     return pl.pallas_call(
-        functools.partial(dispatch_kernel, n, t),
-        out_shape=jax.ShapeDtypeStruct(
-            outgoing.shape[:2] + (outgoing.shape[2] * t,), outgoing.dtype
-        ),
-        in_specs=[pl.BlockSpec(memory_space=pltpu.VMEM)],
-        out_specs=pl.BlockSpec(memory_space=pl.ANY),
+        functools.partial(experts_kernel, n, t),
+        out_shape=[
+            jax.ShapeDtypeStruct((blocks, slots, out), half),
+            jax.ShapeDtypeStruct((length, out), half),
+        ],
+        in_specs=[vmem, vmem] + [anywhere] * 6,
+        out_specs=[anywhere, vmem],
         scratch_shapes=[
+            pltpu.VMEM((blocks, slots, columns * t), half),
+            pltpu.VMEM((blocks, slots, units), half),
+            pltpu.VMEM((blocks, slots, units * t), half),
+            pltpu.VMEM((length, units), half),
+            pltpu.VMEM((length, units * t), half),
+            pltpu.VMEM((blocks, slots, out), half),
+        ]
+        + [pltpu.VMEM(w.shape, half) for w in weights]
+        + [
             pltpu.SemaphoreType.DMA((n,)),
             pltpu.SemaphoreType.DMA((n,)),
             pltpu.SemaphoreType.DMA((t, n)),
             pltpu.SemaphoreType.DMA((t, n)),
-            pltpu.SemaphoreType.DMA((1,)),
+            pltpu.SemaphoreType.DMA((t, n + 1)),
+            pltpu.SemaphoreType.DMA((t, n + 1)),
+            pltpu.SemaphoreType.DMA((n,)),
+            pltpu.SemaphoreType.DMA((n,)),
+            pltpu.SemaphoreType.DMA((n + 9,)),
         ],
-        compiler_params=pltpu.CompilerParams(collective_id=ident, has_side_effects=True),
-        name="dispatch_%d" % ident,
-    )(outgoing)
+        compiler_params=pltpu.CompilerParams(
+            collective_id=ident, has_side_effects=True, vmem_limit_bytes=48 * 1024 * 1024
+        ),
+        name="experts_%d" % ident,
+    )(outgoing, features, *weights)
+
+
+def lowered(hidden, shared, weight, shared_weight):
+    n, t = lax.axis_size("sp"), lax.axis_size("tp")
+    blocks, slots, _ = hidden.shape
+    out = weight.shape[1]
+    hidden_all, shared_all = gather_tp([hidden.reshape(blocks * slots, -1), shared], (1, 1), 0)
+    mine = jnp.dot(hidden_all, weight, preferred_element_type=jnp.float32).astype(jnp.bfloat16)
+    (back,) = swap_sp([mine.reshape(blocks, slots, out)], 0)
+    return back, jnp.dot(
+        shared_all, shared_weight, preferred_element_type=jnp.float32
+    ).astype(jnp.bfloat16)
 
 
 def shards(
@@ -442,26 +574,33 @@
     slots = jnp.arange(experts * capacity, dtype=jnp.int32)
     pick = sum((slots[:, None] == slot[None, :, j]).astype(jnp.bfloat16) for j in range(top))
     outgoing = jnp.dot(pick, features, preferred_element_type=jnp.float32).astype(jnp.bfloat16)
-    arrived = dispatch(outgoing.reshape(experts, capacity, -1), 4)
-    arrived = arrived.reshape(experts * capacity, -1)
-    shared_hidden = (
-        jax.nn.silu(jnp.dot(full_features, common_valve_matrix, preferred_element_type=jnp.float32))
-        * jnp.dot(full_features, common_raising_matrix, preferred_element_type=jnp.float32)
-    ).astype(jnp.bfloat16)
-    expert_hidden = (
-        jax.nn.silu(
-            jnp.dot(arrived, specialist_valve_matrix[0], preferred_element_type=jnp.float32)
+    outgoing = outgoing.reshape(experts, capacity, -1)
+    products = (
+        specialist_valve_matrix[0],
+        specialist_raising_matrix[0],
+        specialist_lowering_matrix[0],
+        common_valve_matrix,
+        common_raising_matrix,
+        common_lowering_matrix,
+    )
+    if small_mesh():
+        returned, shared_out = all_experts(outgoing, full_features, products, 4)
+    else:
+        arrived = dispatch(outgoing).reshape(experts * capacity, -1)
+        gate, up, down, shared_gate, shared_up, shared_down = products
+
+        def hidden_of(rows, one, two):
+            return (
+                jax.nn.silu(jnp.dot(rows, one, preferred_element_type=jnp.float32))
+                * jnp.dot(rows, two, preferred_element_type=jnp.float32)
+            ).astype(jnp.bfloat16)
+
+        returned, shared_out = lowered(
+            hidden_of(arrived, gate, up).reshape(experts, capacity, -1),
+            hidden_of(full_features, shared_gate, shared_up),
+            down,
+            shared_down,
         )
-        * jnp.dot(arrived, specialist_raising_matrix[0], preferred_element_type=jnp.float32)
-    ).astype(jnp.bfloat16)
-    expert_all, shared_all = gather_tp([expert_hidden, shared_hidden], (4, 2), 5)
-    expert_out = jnp.dot(
-        expert_all, specialist_lowering_matrix[0], preferred_element_type=jnp.float32
-    ).astype(jnp.bfloat16)
-    shared_out = jnp.dot(
-        shared_all, common_lowering_matrix, preferred_element_type=jnp.float32
-    ).astype(jnp.bfloat16)
-    (returned,) = swap_sp([expert_out.reshape(experts, capacity, -1)], 6)
     returned = returned.reshape(experts * capacity, -1)
     shares = sum(
         jnp.where(slots[None, :] == slot[:, j, None], specialist_shares[:, j, None], 0.0)

time: 207 us -> 143 us (0.69)
  Pallas kernels: 147 us -> 112 us
  matrix products: 30.3 us -> 8.57 us
  other arithmetic: 13.4 us -> 9.67 us
  local copies, waits for them, and re-layouts: 7.81 us -> 5.02 us
    pallas_call x3 -> x2, Pallas kernels: 55.9 us -> 21.6 us  [gather_tp(): pl.pallas_call(functools.partial(gather_kernel, n, counts), out_shape=[ja...]
    pallas_call x2 -> x1, Pallas kernels: 43.8 us -> 17.3 us  [swap_sp(): pl.pallas_call(functools.partial(swap_kernel, n, select, m), out_shape=[j...]
    pallas_call x1, Pallas kernels: 47.1 us -> 73.5 us  [all_experts(): pl.pallas_call(functools.partial(experts_kernel, n, t), out_shape=[jax.Sh...]
    dot_general x6 -> x0, matrix products: 18.9 us -> none  [the longest x1 6.15 us: shards(): jnp.dot(expert_all, specialist_lowering_matrix[0], preferred_element_type...]
  transfers between devices with their start and end apart: 2 -> 2, of which waited for: 0 -> 0; matrix products, arithmetic and copies ran while one was open for 5% -> 4% of each run, Pallas kernels for 0% -> 0%
where the time goes in v2:
time: 143 us; the launch traced here: 142 us
  Pallas kernels  112 us (78%)
  other arithmetic  9.67 us (7%)
  matrix products  8.57 us (6%)
  starting transfers between devices  6.17 us (4%)
  local copies, waits for them, and re-layouts  5.02 us (4%)
    pallas_call x1, Pallas kernels, all_experts(): pl.pallas_call(functools.partial(experts_kernel, n, t), out_shape=[jax.Sh...  73.5 us
    pallas_call x2, Pallas kernels, gather_tp(): pl.pallas_call(functools.partial(gather_kernel, n, counts), out_shape=[ja...  21.6 us
    pallas_call x1, Pallas kernels, swap_sp(): pl.pallas_call(functools.partial(swap_kernel, n, select, m), out_shape=[j...  17.3 us
    ppermute x1, starting transfers between devices, extended(): lax.ppermute(tail, axis, [(i, (i + 1) % count) for i in range(ends)])  4.88 us
  transfers between devices with their start and end apart: 2, of which 0 were waited for; matrix products, arithmetic and copies ran while one was open for 4% of the time, Pallas kernels for 0%

profile of v2, /device:TPU:0, one launch (start us, length us, event | category | flops | bytes accessed | tf_op | source)
XLA Modules:
  0.0 142.2 jit_solution(2427425909848009177)
XLA Ops:
  0.0 1.0 constant_dynamic-slice_fusion.2
  1.1 0.9 pad_maximum_fusion.1
  2.0 4.9 %collective-permute-start = (bf16[2,512]{1,0:T(2,128)(2,1)S(1)}, bf16[2,512]{1,0:T(2,128)(2,1)S(1)}, u32[]{:S(2)}, u32[]{:S(2)}) collective-permute-start(bf16[2,512]{1,0:T(2,128)(2,1)S(1)} %get-tuple-element.27), channel_id=1, source_target_pairs={{0,4},{4,8},{8,12},{12,16},{16,20},{20,24},{24,28},{1,5},{5,9},{9,... | collective-permute-start | bytes 6152 | tf_op jit(solution)/shard_map/ppermute | solution.py:29
  6.9 1.3 collective-permute-start.1
  8.3 0.7 constant_dynamic-slice_fusion
  9.0 0.7 pad_maximum_fusion.3
  9.7 0.7 exponential_negate_fusion
  10.4 0.8 multiply_add_fusion
  11.3 0.2 fusion.49
  11.5 0.2 slice_reduce_fusion.4
  11.8 1.0 convert_multiply_fusion.3
  13.7 0.5 multiply_convert_fusion.3
  14.3 0.2 fusion.53
  14.7 0.9 convolution_convert_fusion.1
  15.6 0.7 broadcast_in_dim.159.refs_1_
  16.3 17.3 %swap_sp_1.1 = (bf16[8,256,128]{2,1,0:T(8,128)(2,1)}, f32[8,4,128]{2,1,0:T(4,128)}) custom-call(bf16[2,256,128]{2,1,0:T(8,128)(2,1)} %bitcast.116, f32[2,4,128]{2,1,0:T(4,128)} %broadcast_in_dim.159.refs_1_), custom_call_target="tpu_custom_call" | custom-call | tf_op jit(solution)/shard_map/swap_sp_1/pallas_call | solution.py:182
  33.6 0.8 copy.45
  34.6 1.2 bitcast_convert_fusion
  35.8 0.2 multiply_reduce_fusion
  36.0 0.2 convolution_bitcast_fusion
  36.3 1.7 %multiply_reduce_fusion.1 = (f32[320]{0:T(512)S(1)}, f32[320,4,64]{0,2,1:T(8,128)S(1)}) fusion(f32[320,4,64]{0,2,1:T(8,128)S(1)} %bitcast.117, bf16[320,4,64]{0,2,1:T(8,128)(2,1)S(1)} %bitcast.115, f32[4]{0:T(128)S(1)} %copy-done.11, f32[2,320,4,64]{1,3,2,0:T(8,128)S(1)} %convolution_bitcast_fusion, f32[320,4]{0,1:T(4,128)S(1)} %get-tuple-element.29, ...), kind=kOutput, calls=%fused_computation.63 | convolution fusion | flops 57753280 | bytes 2688768 | tf_op jit(solution)/shard_map/hts,shp->thp/dot_general | solution.py:501
  38.1 0.8 multiply_convert_fusion.5.refs_0_
  38.9 9.0 %gather_tp_2.1 = (bf16[320,1024]{1,0:T(8,128)(2,1)}, f32[1,2048]{1,0:T(1,128)}) custom-call(bf16[320,256]{1,0:T(8,128)(2,1)} %multiply_convert_fusion.5.refs_0_, f32[1,512]{1,0:T(1,128)} %bitcast.127), custom_call_target="tpu_custom_call" | custom-call | tf_op jit(solution)/shard_map/gather_tp_2/pallas_call | solution.py:127
  47.9 2.3 %fusion.7.refs_0_ = bf16[320,512]{1,0:T(8,128)(2,1)} fusion(bf16[320,1024]{1,0:T(8,128)(2,1)} %get-tuple-element.13, bf16[1024,512]{1,0:T(8,128)(2,1)S(1)} %copy-done, bf16[320,512]{1,0:T(8,128)(2,1)S(1)} %copy-done.10), kind=kOutput, calls=%fused_computation.21 | convolution fusion | flops 336035840 | bytes 2359296 | tf_op jit(solution)/shard_map/dot_general | solution.py:554
  50.2 12.6 %gather_tp_3.1 = bf16[320,2048]{1,0:T(8,128)(2,1)} custom-call(bf16[320,512]{1,0:T(8,128)(2,1)} %fusion.7.refs_0_), custom_call_target="tpu_custom_call" | custom-call | tf_op jit(solution)/shard_map/gather_tp_3/pallas_call | solution.py:127
  62.9 1.8 %fusion = f32[320]{0:T(512)S(1)} fusion(bf16[320,2048]{1,0:T(8,128)(2,1)} %gather_tp_3.1), kind=kLoop, calls=%fused_computation.2 | loop fusion | flops 1965760 | bytes 1312000 | tf_op jit(solution)/shard_map/reduce_sum | solution.py:559
  64.7 0.4 fusion.2.feats
  65.1 0.8 convolution_convert_fusion
  65.9 0.8 copy-done.1
  66.6 73.5 %experts_4.1 = (bf16[8,120,512]{2,1,0:T(8,128)(2,1)S(1)}, bf16[320,512]{1,0:T(8,128)(2,1)S(1)}) custom-call(bf16[8,120,512]{2,1,0:T(8,128)(2,1)S(1)} %bitcast.110, bf16[320,2048]{1,0:T(8,128)(2,1)S(1)} %fusion.2.feats, bf16[2048,512]{1,0:T(8,128)(2,1)S(1)} %bitcast.109, bf16[2048,512]{1,0:T(8,128)(2,1)} %bitcast.113, bf16[2048,512]{1,0:T(8,128)(2,1)} %bitcast.114, ...), custom_call_target="tpu_custom_call" | custom-call | tf_op jit(solution)/shard_map/experts_4/pallas_call | solution.py:369
  140.2 0.6 fusion.35
  140.8 1.4 fusion.8
  (55 shorter events, 1.6 us)
Async XLA Ops:
  0.0 47.9 %copy-start = (bf16[1024,512]{1,0:T(8,128)(2,1)S(1)}, bf16[1024,512]{1,0:T(8,128)(2,1)}, u32[]{:S(2)}) copy-start(bf16[1024,512]{1,0:T(8,128)(2,1)} %param.38) | copy-start | bytes 3145732
  0.0 13.6 %copy-start.3 = (bf16[320,256]{1,0:T(8,128)(2,1)S(1)}, bf16[320,256]{1,0:T(8,128)(2,1)}, u32[]{:S(2)}) copy-start(bf16[320,256]{1,0:T(8,128)(2,1)} %param.25) | copy-start | bytes 491524
  0.0 12.8 %copy-start.5 = (s32[320,2]{0,1:T(2,128)S(1)}, s32[320,2]{0,1:T(2,128)}, u32[]{:S(2)}) copy-start(s32[320,2]{0,1:T(2,128)} %param.40) | copy-start | bytes 7684
  0.0 13.1 %copy-start.7 = (f32[320,2]{0,1:T(2,128)S(1)}, f32[320,2]{0,1:T(2,128)}, u32[]{:S(2)}) copy-start(f32[320,2]{0,1:T(2,128)} %param.41) | copy-start | bytes 7684
  2.0 11.5 %collective-permute-start = (bf16[2,512]{1,0:T(2,128)(2,1)S(1)}, bf16[2,512]{1,0:T(2,128)(2,1)S(1)}, u32[]{:S(2)}, u32[]{:S(2)}) collective-permute-start(bf16[2,512]{1,0:T(2,128)(2,1)S(1)} %get-tuple-element.27), channel_id=1, source_target_pairs={{0,4},{4,8},{8,12},{12,16},{16,20},{20,24},{24,28},{1,5},{5,9},{9,... | collective-permute-start | bytes 6152 | tf_op jit(solution)/shard_map/ppermute | solution.py:29
  6.9 6.6 %collective-permute-start.1 = (bf16[2,512]{1,0:T(2,128)(2,1)S(1)}, bf16[2,512]{1,0:T(2,128)(2,1)S(1)}, u32[]{:S(2)}, u32[]{:S(2)}) collective-permute-start(bf16[2,512]{1,0:T(2,128)(2,1)S(1)} %get-tuple-element.28), channel_id=1, source_target_pairs={{4,0},{8,4},{12,8},{16,12},{20,16},{24,20},{28,24},{5,1},{9,5},{13... | collective-permute-start | bytes 6152 | tf_op jit(solution)/shard_map/ppermute | solution.py:31
  16.3 20.0 %copy-start.11 = (f32[4]{0:T(128)S(1)}, f32[4]{0:T(128)}, u32[]{:S(2)}) copy-start(f32[4]{0:T(128)} %param.33) | copy-start | bytes 52
  36.2 1.9 %copy-start.9 = (f32[256]{0:T(256)S(1)}, f32[256]{0:T(256)}, u32[]{:S(2)}) copy-start(f32[256]{0:T(256)} %param.37) | copy-start | bytes 3076
  36.3 11.6 %copy-start.10 = (bf16[320,512]{1,0:T(8,128)(2,1)S(1)}, bf16[320,512]{1,0:T(8,128)(2,1)}, u32[]{:S(2)}) copy-start(bf16[320,512]{1,0:T(8,128)(2,1)} %param.24) | copy-start | bytes 983044
  50.2 14.4 %copy-start.6 = (f32[1,2048]{1,0:T(1,128)S(1)}, f32[1,2048]{1,0:T(1,128)}, u32[]{:S(2)}) copy-start(f32[1,2048]{1,0:T(1,128)} %get-tuple-element.14) | copy-start | bytes 24580
  62.8 1.8 %copy-start.2 = (bf16[320,2048]{1,0:T(8,128)(2,1)S(1)}, bf16[320,2048]{1,0:T(8,128)(2,1)}, u32[]{:S(2)}) copy-start(bf16[320,2048]{1,0:T(8,128)(2,1)} %gather_tp_3.1) | copy-start | bytes 3932164
  62.8 2.2 %copy-start.4 = (bf16[320,512]{1,0:T(8,128)(2,1)S(1)}, bf16[320,512]{1,0:T(8,128)(2,1)}, u32[]{:S(2)}) copy-start(bf16[320,512]{1,0:T(8,128)(2,1)} %fusion.7.refs_0_) | copy-start | bytes 983044
  62.8 2.2 %copy-start.8 = (f32[512]{0:T(512)S(1)}, f32[512]{0:T(512)}, u32[]{:S(2)}) copy-start(f32[512]{0:T(512)} %param.39) | copy-start | bytes 6148
  65.1 1.6 %copy-start.1 = (bf16[1,2048,512]{2,1,0:T(8,128)(2,1)S(1)}, bf16[1,2048,512]{2,1,0:T(8,128)(2,1)}, u32[]{:S(2)}) copy-start(bf16[1,2048,512]{2,1,0:T(8,128)(2,1)} %param.42) | copy-start | bytes 6291460
